TPU v7x, 256 devices: a whole 4x4x8 slice. The times are simulated.
256 devices in a mesh: sp: 64 (over z, y, core), tp: 4 (over x).
Axes of the slice: x: 4, y: 4, z: 8, core: 2. Of those that a mesh axis runs over, the one named last changes fastest.
Arguments:
- tokens: bfloat16 [16384, 2048], P(('sp', 'tp')), may hold values from -6 to 6
- norm_gain: float32 [2048], replicated, may hold values from 0.1 to 6, as said below
- query_weight: bfloat16 [2048, 16, 128], P(None, 'tp'), may hold values from -0.21875 to 0.21875
- key_weight: bfloat16 [2048, 4, 128], P(None, 'tp'), may hold values from -0.125 to 0.125
- value_weight: bfloat16 [2048, 4, 128], P(None, 'tp'), may hold values from -0.125 to 0.125
- mix_lambda: float32 [16], P('tp'), may hold values from 0.3 to 0.8
- head_gain: float32 [128], replicated, may hold values from 0.1 to 1.9
- pool_weight: bfloat16 [2048, 4, 512], P(None, 'tp'), may hold values from -0.125 to 0.125
- pool_mix: bfloat16 [4, 512, 512], P('tp'), may hold values from -0.25 to 0.25
- pool_scale: float32 [4, 512], P('tp'), may hold values from 0.1 to 1.9
- gate_weight: bfloat16 [2048, 2, 2048], P(None, None, 'tp'), may hold values from -0.125 to 0.125
- out_weight: bfloat16 [2048, 2048], P('tp'), may hold values from -0.125 to 0.125
Outputs:
- mixed: bfloat16 [16384, 2048], P(('sp', 'tp'))
- log_sums: float32 [2, 16, 16384], P(None, 'tp', 'sp')
Inputs may be any that keep to these rules, and one draw needn't show every extreme that they name: `norm_gain`: positive.
All inputs are finite; a program needn't handle non-finite values.
Results may differ from a plain program's by a relative error of at most 0.013.
Values may be sent and summed in bfloat16 or wider, within the bound.
A program may use at most 128 MiB of HBM per device.

v0:
```python
import math

import jax
import jax.numpy as jnp
from jax import lax
from jax.sharding import PartitionSpec as P

WINDOW = 16


NORM_EPS = 1e-06


def copy_for_each(array, axis):
    size = lax.axis_size(axis)
    return lax.all_to_all(
        jnp.broadcast_to(array[None], (size, *array.shape)), axis, 0, 0, tiled=True
    )


def laid_out(pieces, dim):
    shape = list(pieces.shape[1:])
    shape[dim] *= pieces.shape[0]
    return jnp.moveaxis(pieces, 0, dim).reshape(shape)


def collect(array, axis, dim):
    pieces = copy_for_each(array, axis)
    return laid_out(pieces, dim)


def sent_together(arrays, axis, dim, along):
    ends, at = ([], 0)
    for a in arrays[:-1]:
        at += a.shape[along]
        ends.append(at)
    both = jnp.concatenate(arrays, axis=along)
    return tuple(jnp.split(lax.all_gather(both, axis, axis=dim, tiled=True), ends, axis=along))


def shifted(block, axis, distance):
    devices = range(lax.axis_size(axis))
    route = [(i - distance, i) for i in devices if i - distance in devices]
    return lax.ppermute(block, axis, route)


def cut_along(array, dim, size):
    before, after = (array.shape[:dim], array.shape[dim + 1 :])
    return jnp.moveaxis(array.reshape(*before, size, -1, *after), dim, 0)


def sent_and_summed(array, axis, dim):
    size = lax.axis_size(axis)
    pieces = lax.all_to_all(cut_along(array, dim, size), axis, 0, 0, tiled=True)
    return jnp.sum(pieces.astype(jnp.float32), axis=0)


def attend(
    queries, key_buffer, value_buffer, key_start, query_start, weight_lambda, head_dim, value_dim
):
    tok_rows, kv_local, group_size = (queries.shape[0], queries.shape[1], queries.shape[2])
    total_keys = key_buffer.shape[0]
    block_keys = math.gcd(total_keys, 512)
    keys_split = key_buffer.reshape(total_keys, kv_local, 2, head_dim)
    values_split = value_buffer.reshape(total_keys, kv_local, value_dim)
    query_pos = query_start + jnp.arange(tok_rows, dtype=jnp.int32)
    score_scale = head_dim ** (-0.5)
    low_index = jnp.maximum(0, -key_start)
    high_index = query_start + tok_rows
    first_block = low_index // block_keys
    last_block = (high_index + block_keys - 1) // block_keys

    def online_step(block_index, carry):
        running_max, running_sum, accum = carry
        key_begin = block_index * block_keys
        block_keys_arr = lax.dynamic_slice_in_dim(keys_split, key_begin, block_keys, 0)
        scores = (
            jnp.einsum(
                "qgrmd,kgmd->grmqk", queries, block_keys_arr, preferred_element_type=jnp.float32
            )
            * score_scale
        )
        key_pos = key_begin + jnp.arange(block_keys, dtype=jnp.int32)
        visible = (key_pos[None, :] <= query_pos[:, None]) & (key_pos[None, :] >= 0)
        block_max = jnp.max(jnp.where(visible, scores, -1e30), axis=4)
        new_max = jnp.maximum(running_max, block_max)
        rescale = jnp.exp(running_max - new_max)
        probs = jnp.where(visible, jnp.exp(scores - new_max[..., None]), 0.0)
        new_sum = running_sum * rescale + jnp.sum(probs, axis=4)
        block_values = lax.dynamic_slice_in_dim(values_split, key_begin, block_keys, 0)
        new_accum = accum * rescale[..., None] + jnp.einsum(
            "grmqk,kgd->grmqd",
            probs.astype(jnp.bfloat16),
            block_values,
            preferred_element_type=jnp.float32,
        )
        return (new_max, new_sum, new_accum)

    start_carry = (
        jnp.full((kv_local, group_size, 2, tok_rows), -1e30, jnp.float32),
        jnp.zeros((kv_local, group_size, 2, tok_rows), jnp.float32),
        jnp.zeros((kv_local, group_size, 2, tok_rows, value_dim), jnp.float32),
    )
    running_max, running_sum, accum = lax.fori_loop(
        first_block, last_block, online_step, start_carry
    )
    first_map = accum[:, :, 0] / running_sum[:, :, 0, :, None]
    second_map = accum[:, :, 1] / running_sum[:, :, 1, :, None]
    head_out = first_map - weight_lambda[:, :, None, None] * second_map
    log_sums = running_max + jnp.log(running_sum)
    return (head_out, log_sums)


def finish_heads(head_out, log_sums, head_gain, heads_local, value_dim):
    tok_rows = head_out.shape[2]
    head_outs = head_out.reshape(heads_local, tok_rows, value_dim)
    normed_heads = (
        head_outs
        * lax.rsqrt(jnp.mean(head_outs * head_outs, axis=2, keepdims=True) + NORM_EPS)
        * head_gain
    )
    attended = jnp.transpose(normed_heads, (1, 0, 2)).reshape(tok_rows, heads_local * value_dim)
    log_out = jnp.transpose(log_sums.reshape(heads_local, 2, tok_rows), (1, 0, 2))
    return (attended, log_out)


def local(
    tokens,
    norm_gain,
    query_weight,
    key_weight,
    value_weight,
    mix_lambda,
    head_gain,
    pool_weight,
    pool_mix,
    pool_scale,
    gate_weight,
    out_weight,
):
    model_width = tokens.shape[1]
    heads_local = query_weight.shape[1]
    kv_local = key_weight.shape[1]
    head_dim = query_weight.shape[2] // 2
    value_dim = value_weight.shape[2]
    groups_local = pool_weight.shape[1]
    group_width = pool_weight.shape[2]
    channels = gate_weight.shape[2]
    matrices = (
        query_weight.reshape(model_width, -1),
        key_weight.reshape(model_width, -1),
        value_weight.reshape(model_width, -1),
        pool_weight.reshape(model_width, -1),
        gate_weight.reshape(model_width, -1),
    )

    def project(rows_piece):
        inputs = rows_piece.astype(jnp.float32)
        normed = (
            inputs
            * lax.rsqrt(jnp.mean(inputs * inputs, axis=1, keepdims=True) + NORM_EPS)
            * norm_gain
        ).astype(jnp.bfloat16)
        return jnp.concatenate(
            [
                jnp.dot(normed, matrix, preferred_element_type=jnp.float32).astype(jnp.bfloat16)
                for matrix in matrices
            ],
            axis=1,
        )

    joined = project(collect(tokens, "tp", 0))
    tok_rows = joined.shape[0]
    bounds = [0]
    for matrix in matrices:
        bounds.append(bounds[-1] + matrix.shape[1])
    queries = joined[:, bounds[0] : bounds[1]].reshape(
        tok_rows, kv_local, heads_local // kv_local, 2, head_dim
    )
    keys_own = joined[:, bounds[1] : bounds[2]]
    values_own = joined[:, bounds[2] : bounds[3]]
    pool_in = joined[:, bounds[3] : bounds[4]]
    gate_pre = joined[:, bounds[4] : bounds[5]].reshape(tok_rows, 2, channels)
    rim_rows = pool_in[tok_rows - WINDOW :]
    seq_index = lax.axis_index("sp")
    query_start = seq_index * tok_rows
    key_buffer, value_buffer = sent_together((keys_own, values_own), "sp", 0, 1)
    rim_prev = shifted(rim_rows, "sp", 1)
    key_start = jnp.int32(0)
    lambda_local = mix_lambda.reshape(kv_local, heads_local // kv_local)
    head_out, log_sums = attend(
        queries, key_buffer, value_buffer, key_start, query_start, lambda_local, head_dim, value_dim
    )
    attended, log_out = finish_heads(head_out, log_sums, head_gain, heads_local, value_dim)
    positions = query_start + jnp.arange(tok_rows, dtype=jnp.int32)
    pool_split = pool_in.reshape(tok_rows, groups_local, group_width)
    extended = (
        jnp.concatenate([rim_prev, pool_in], axis=0)
        .astype(jnp.float32)
        .reshape(WINDOW + tok_rows, groups_local, group_width)
    )
    group_index = lax.axis_index("tp") * groups_local + 0
    window_span = jnp.left_shift(jnp.int32(2), group_index)
    window_sum = jnp.zeros((tok_rows, group_width), jnp.float32)
    for back_rows in range(WINDOW):
        window_sum = window_sum + jnp.where(
            back_rows < window_span,
            extended[WINDOW - back_rows : WINDOW - back_rows + tok_rows, 0],
            0.0,
        )
    counts = jnp.minimum(positions + 1, window_span).astype(jnp.float32)
    means = window_sum / counts[:, None]
    pooled = (means - pool_split[:, 0].astype(jnp.float32)).astype(jnp.bfloat16)
    group_parts = jnp.dot(pooled, pool_mix[0], preferred_element_type=jnp.float32) * pool_scale[0]
    merged = (
        jax.nn.sigmoid(gate_pre[:, 0].astype(jnp.float32)) * attended
        + jax.nn.sigmoid(gate_pre[:, 1].astype(jnp.float32)) * group_parts
    ).astype(jnp.bfloat16)
    mixed = sent_and_summed(
        jnp.dot(merged, out_weight, preferred_element_type=jnp.float32).astype(jnp.bfloat16),
        "tp",
        0,
    )
    return (mixed.astype(jnp.bfloat16), log_out)


def solution(mesh):
    in_specs = (
        P(("sp", "tp"), None),
        P(),
        P(None, "tp", None),
        P(None, "tp", None),
        P(None, "tp", None),
        P("tp"),
        P(),
        P(None, "tp", None),
        P("tp", None, None),
        P("tp", None),
        P(None, None, "tp"),
        P("tp", None),
    )
    out_specs = (P(("sp", "tp"), None), P(None, "tp", "sp"))
    return jax.shard_map(local, mesh=mesh, in_specs=in_specs, out_specs=out_specs, check_vma=False)
```

profile of v0, /device:TPU:248, one launch (start us, length us, event | category | flops | bytes accessed | tf_op | source)
XLA Modules:
  0.0 330.0 jit_solution(275592292067196041)
XLA Ops:
  8.5 19.2 %all_to_all.10 = bf16[4,64,2048]{2,1,0:T(8,128)(2,1)S(1)} all-to-all(bf16[4,64,2048]{2,1,0:T(8,128)(2,1)S(1)} %broadcast_in_dim.56), channel_id=1, replica_groups=mesh['sp'=64,'tp'=4] {'tp'}, dimensions={0} | all-to-all | bytes 2097152 | tf_op jit(solution)/shard_map/all_to_all | solution.py:16
  30.0 5.3 %copy.48 = bf16[256,8,2,512]{3,1,2,0:T(8,128)(2,1)} copy(bf16[256,8,2,512]{3,2,1,0:T(2,128)(2,1)} %bitcast.152) | data formatting | bytes 8388608
  35.4 2.3 fusion.36
  39.6 4.3 %convolution_convert_fusion.1 = bf16[256,1024]{1,0:T(8,128)(2,1)} fusion(bf16[256,2048]{1,0:T(8,128)(2,1)S(1)} %bitcast.149, bf16[2048,1024]{1,0:T(8,128)(2,1)} %bitcast.153), kind=kOutput, calls=%fused_computation.41 | convolution fusion | flops 1074003968 | bytes 5767168 | tf_op jit(solution)/shard_map/dot_general | solution.py:166
  46.3 3.1 fusion.39
  53.1 60.7 %all-gather.2.cloned.1.call-done = bf16[16384,256]{0,1:T(8,128)(2,1)} async-done(((bf16[256,256]{0,1:T(8,128)(2,1)}), bf16[16384,256]{0,1:T(8,128)(2,1)}) %all-gather.2.cloned.1.call-update) | async-done | bytes 8388624 | tf_op jit(solution)/shard_map/all_gather | solution.py:38
  113.7 5.8 %slice_bitcast_fusion = (bf16[16384,1,128]{0,2,1:T(8,128)(2,1)}, bf16[16384,128]{0,1:T(8,128)(2,1)}) fusion(bf16[16384,256]{0,1:T(8,128)(2,1)} %all-gather.2.cloned.1.call-done), kind=kLoop, calls=%fused_computation.29 | loop fusion | bytes 16777216 | tf_op jit(solution)/shard_map/reshape | solution.py:65
  119.6 170.0 %while.15 = (s32[]{:T(128)}, f32[1,4,2,256]{3,1,2,0:T(4,128)S(1)}, f32[1,4,2,256]{3,1,2,0:T(4,128)S(1)}, f32[1,4,2,256,128]{4,3,2,1,0:T(8,128)S(1)}, s32[]{:T(12...) while((s32[]{:T(128)}, f32[1,4,2,256]{3,1,2,0:T(4,128)S(1)}, ...), condition=%wide.region_4.5_spmd.clone, body=%wide.region_1.4_spmd.clone.sunk | while | flops 411836160 | bytes 15744191 | solution.py:104
  127.9 2.3 fusion.144
  133.2 2.3 fusion.144
  138.5 2.3 fusion.144
  143.8 2.3 fusion.144
  154.4 2.3 fusion.144
  159.7 2.3 fusion.144
  165.0 2.3 fusion.144
  170.4 2.3 fusion.144
  175.7 2.3 fusion.144
  186.3 2.3 fusion.144
  191.6 2.3 fusion.144
  196.9 2.3 fusion.144
  202.2 2.3 fusion.144
  207.5 2.3 fusion.144
  212.8 2.3 fusion.144
  223.4 2.3 fusion.144
  228.7 2.3 fusion.144
  234.0 2.3 fusion.144
  239.3 2.3 fusion.144
  244.6 2.3 fusion.144
  255.2 2.3 fusion.144
  292.6 9.9 %convolution_convert_fusion = bf16[256,2048]{1,0:T(8,128)(2,1)} fusion(bf16[512,2048]{1,0:T(8,128)(2,1)S(1)} %copy-done, bf16[1,512,512]{2,1,0:T(8,128)(2,1)} %param.22, f32[256,512]{1,0:T(8,128)S(1)} %copy.39, bf16[256,512]{1,0:T(8,128)(2,1)} %copy-done.4, f32[272,512]{1,0:T(8,128)} %maximum_convert_fusion, bf16[256,1,512]{2,1,0:T(2,128)(2,1)} %get-tuple-element.133, ...), kind=kOutput, calls=%fused_computation.32 | convolution fusion | flops 677904384 | bytes 13896720 | tf_op jit(solution)/shard_map/dot_general | solution.py:220
  302.5 4.2 %all-to-all-start.1 = ((bf16[4,64,2048]{2,1,0:T(8,128)(2,1)}), bf16[4,64,2048]{2,1,0:T(8,128)(2,1)S(1)}, u32[]{:S(2)}, u32[]{:S(2)}) async-start(bf16[4,64,2048]{2,1,0:T(8,128)(2,1)} %bitcast.156), calls=%async_computation.1 | async-start | bytes 2097152 | tf_op jit(solution)/shard_map/all_to_all | solution.py:54
  307.4 14.9 %all-to-all-done.1 = bf16[4,64,2048]{2,1,0:T(8,128)(2,1)S(1)} async-done(((bf16[4,64,2048]{2,1,0:T(8,128)(2,1)}), bf16[4,64,2048]{2,1,0:T(8,128)(2,1)S(1)}, u32[]{:S(2)}, u32[]{:S(2)}) %all-to-all-start.1) | async-done | bytes 1048608 | tf_op jit(solution)/shard_map/all_to_all | solution.py:54
  (378 shorter events, 134.8 us)
Async XLA Ops:
  7.2 285.4 %copy-start = (bf16[512,2048]{1,0:T(8,128)(2,1)S(1)}, bf16[512,2048]{1,0:T(8,128)(2,1)}, u32[]{:S(2)}) copy-start(bf16[512,2048]{1,0:T(8,128)(2,1)} %param.25) | copy-start | bytes 6291460
  7.2 20.8 %copy-start.5 = (f32[2048]{0:T(1024)S(1)}, f32[2048]{0:T(1024)}, u32[]{:S(2)}) copy-start(f32[2048]{0:T(1024)} %param.15) | copy-start | bytes 24580
  7.2 106.5 %all-gather.2.cloned.1.call-start = ((), (), s32[]{:S(2)}) async-start(), calls=%async_computation.2 | async-start | bytes 8519680 | tf_op jit(solution)/shard_map/all_gather | solution.py:38
  7.2 21.1 %copy-start.2 = (bf16[2048,1,128]{2,0,1:T(8,128)(2,1)S(1)}, bf16[2048,1,128]{2,0,1:T(8,128)(2,1)}, u32[]{:S(2)}) copy-start(bf16[2048,1,128]{2,0,1:T(8,128)(2,1)} %param.18) | copy-start | bytes 1572868
  7.2 21.6 %copy-start.3 = (bf16[2048,1,128]{2,0,1:T(8,128)(2,1)S(1)}, bf16[2048,1,128]{2,0,1:T(8,128)(2,1)}, u32[]{:S(2)}) copy-start(bf16[2048,1,128]{2,0,1:T(8,128)(2,1)} %param.17) | copy-start | bytes 1572868
  37.7 14.5 %copy-start.4 = (bf16[256,512]{1,0:T(8,128)(2,1)}, bf16[256,512]{1,0:T(8,128)(2,1)S(1)}, u32[]{:S(2)}) copy-start(bf16[256,512]{1,0:T(8,128)(2,1)S(1)} %fusion.36) | copy-start | bytes 786436
  37.7 14.4 %collective-permute-start = (bf16[16,512]{1,0:T(8,128)(2,1)S(1)}, bf16[16,512]{1,0:T(8,128)(2,1)S(1)}, u32[]{:S(2)}, u32[]{:S(2)}) collective-permute-start(bf16[16,512]{1,0:T(8,128)(2,1)S(1)} %slice.112), channel_id=1, source_target_pairs={{0,4},{4,8},{8,12},{12,16},{16,20},{20,24},{24,28},{28,32},{32,36}... | collective-permute-start | bytes 49160 | tf_op jit(solution)/shard_map/ppermute | solution.py:44
  46.2 3.1 copy-start.1
  119.6 171.3 %copy-start.6 = (f32[4]{0:T(128)S(1)}, f32[4]{0:T(128)}, u32[]{:S(2)}) copy-start(f32[4]{0:T(128)} %param.19) | copy-start | bytes 52
  119.6 172.7 %copy-start.7 = (f32[128]{0:T(128)S(1)}, f32[128]{0:T(128)}, u32[]{:S(2)}) copy-start(f32[128]{0:T(128)} %param.20) | copy-start | bytes 1540
  289.6 3.0 copy-start.8
  302.5 19.8 %all-to-all-start.1 = ((bf16[4,64,2048]{2,1,0:T(8,128)(2,1)}), bf16[4,64,2048]{2,1,0:T(8,128)(2,1)S(1)}, u32[]{:S(2)}, u32[]{:S(2)}) async-start(bf16[4,64,2048]{2,1,0:T(8,128)(2,1)} %bitcast.156), calls=%async_computation.1 | async-start | bytes 2097152 | tf_op jit(solution)/shard_map/all_to_all | solution.py:54
Sparse Core Ops, SparseCore 0:
  30.1 83.5 all-gather.1
where the time goes:
time: 332 us; the launch traced here: 330 us
  matrix products  149 us (45%)
  waiting for transfers between devices  75.6 us (23%)
  other arithmetic  43.5 us (13%)
  local copies, waits for them, and re-layouts  19.3 us (6%)
  blocking collectives  19.2 us (6%)
  between operations  14.3 us (4%)
  starting transfers between devices  6.2 us (2%)
    dot_general x32, matrix products, online_step(): jnp.einsum('grmqk,kgd->grmqd', probs.astype(jnp.bfloat16), block_values,...  73.1 us
    all_gather x1, waiting for transfers between devices, sent_together(): lax.all_gather(both, axis, axis=dim, tiled=True)  60.7 us
    dot_general x32, matrix products, online_step(): jnp.einsum('qgrmd,kgmd->grmqk', queries, block_keys_arr, preferred_elemen...  55 us
    another operation x32, other arithmetic  30.4 us
    all_to_all x1, blocking collectives, copy_for_each(): lax.all_to_all(jnp.broadcast_to(array[None], (size, *array.shape)), axis,...  19.2 us
    all_to_all x1, waiting for transfers between devices, sent_and_summed(): pieces = lax.all_to_all(cut_along(array, dim, size), axis, 0, 0, tiled=True)  14.9 us
    dot_general x5, matrix products, project(): jnp.dot(normed, matrix, preferred_element_type=jnp.float32)  10.7 us
    dot_general x1, matrix products, local(): jnp.dot(merged, out_weight, preferred_element_type=jnp.float32)  9.88 us
  transfers between devices with their start and end apart: 3, of which 2 were waited for; matrix products, arithmetic and copies ran while one was open for 7% of the time, Pallas kernels for 0%

commit v1 on v0

v1 whole, which is shorter than its diff:
```python
import functools

import jax
import jax.numpy as jnp
from jax import lax
from jax.experimental import pallas as pl
from jax.experimental.pallas import tpu as pltpu
from jax.sharding import PartitionSpec as P

WINDOW = 16
NORM_EPS = 1e-06
MESH = pl.DeviceIdType.MESH
NEG = -1e30
NZ, NY, NC = 8, 4, 2
LAG, NB = 2, 4
ROWS = 256
HALF = 128
KB = 512


def copy_for_each(array, axis):
    size = lax.axis_size(axis)
    return lax.all_to_all(
        jnp.broadcast_to(array[None], (size, *array.shape)), axis, 0, 0, tiled=True
    )


def shifted(block, axis, distance):
    devices = range(lax.axis_size(axis))
    route = [(i - distance, i) for i in devices if i - distance in devices]
    return lax.ppermute(block, axis, route)


def sent_and_summed(array, axis):
    size = lax.axis_size(axis)
    pieces = lax.all_to_all(array.reshape(size, -1, array.shape[1]), axis, 0, 0, tiled=True)
    return jnp.sum(pieces.astype(jnp.float32), axis=0)


def attention_kernel(
    q_ref, qs_ref, k_ref, v_ref, lam_ref, gain_ref,
    att_ref, lse_ref,
    gk, gv, qbd, qin, m_ref, acc_ref, attx, lsex, attr, lser,
    *rest,
):
    sb, pb, bm = rest[:NB], rest[NB:2 * NB], rest[2 * NB:3 * NB]
    (own_sem, ky_s, ky_r, vy_s, vy_r, kz_s, kz_r, vz_s, vz_r,
     sk_s, sk_r, sv_s, sv_r, q_s, q_r, o_s, o_r) = rest[3 * NB:]
    me = lax.axis_index("sp")
    z, y, c = me // (NY * NC), (me // NC) % NY, me % NC

    def at(zz, yy, cc):
        return {"sp": (zz * NY + yy) * NC + cc}

    sibling = at(z, y, 1 - c)
    partner = at(NZ - 1 - z, NY - 1 - y, c)
    z_up, z_down = at((z + 1) % NZ, y, c), at((z + NZ - 1) % NZ, y, c)
    y_peers = [at(z, (y + d) % NY, c) for d in (1, 2, 3)]

    barrier = pltpu.get_barrier_semaphore()
    peers = [sibling, partner, z_up, z_down, *y_peers]
    for peer in peers:
        pl.semaphore_signal(barrier, inc=1, device_id=peer, device_id_type=MESH)
    pl.semaphore_wait(barrier, len(peers))

    def remote(src, dst, s, r, dev):
        return pltpu.make_async_remote_copy(
            src_ref=src, dst_ref=dst, send_sem=s, recv_sem=r,
            device_id=dev, device_id_type=MESH,
        )

    def slab(j):
        k = (j + 1) // 2
        return lax.rem(z + NZ + jnp.where(lax.rem(j, 2) == 1, -k, k), NZ)

    def k_to_y(j, d):
        zs = slab(j)
        return remote(gk.at[zs, c, y], gk.at[zs, c, y], ky_s.at[j, d], ky_r.at[j, d], y_peers[d])

    def k_from_y(j, d):
        zs, yy = slab(j), lax.rem(y + NY - (d + 1), NY)
        return remote(gk.at[zs, c, yy], gk.at[zs, c, yy], ky_s.at[j, d], ky_r.at[j, d], y_peers[d])

    def v_to_y(d):
        return remote(v_ref, gv.at[z, c, y], vy_s.at[d], vy_r.at[d], y_peers[d])

    def v_from_y(d):
        yy = lax.rem(y + NY - (d + 1), NY)
        return remote(v_ref, gv.at[z, c, yy], vy_s.at[d], vy_r.at[d], y_peers[d])

    def to_z(j, zs):
        dev = {"sp": jnp.where(lax.rem(j, 2) == 1, z_up["sp"], z_down["sp"])}
        return (
            remote(gk.at[zs, c, y], gk.at[zs, c, y], kz_s.at[j], kz_r.at[j], dev),
            remote(gv.at[zs, c], gv.at[zs, c], vz_s.at[j], vz_r.at[j], dev),
        )

    def to_sibling(j, cc):
        zs = slab(j)
        return (
            remote(gk.at[zs, cc], gk.at[zs, cc], sk_s.at[j], sk_r.at[j], sibling),
            remote(gv.at[zs, cc], gv.at[zs, cc], sv_s.at[j], sv_r.at[j], sibling),
        )

    q_copy = remote(qs_ref, qin, q_s, q_r, partner)
    q_copy.start()
    own_k = pltpu.make_async_copy(k_ref, gk.at[z, c, y], own_sem.at[0])
    own_v = pltpu.make_async_copy(v_ref, gv.at[z, c, y], own_sem.at[1])
    own_k.start()
    own_v.start()
    for d in range(3):
        v_to_y(d).start()
    own_k.wait()
    for d in range(3):
        k_to_y(0, d).start()
    own_v.wait()

    m_ref[...] = jnp.full_like(m_ref, NEG)
    acc_ref[...] = jnp.zeros_like(acc_ref)
    is_low = z < NZ // 2
    g_own = jnp.where(is_low, 0, 4)
    g_far = 4 - g_own

    def block_diagonal(q):
        top = lax.broadcasted_iota(jnp.int32, (HALF, HALF), 0) < 64
        zero = jnp.zeros_like(q)
        return jnp.concatenate([jnp.where(top, q, zero), jnp.where(top, zero, q)], axis=1)

    for h in range(4):
        qbd[g_own + h] = block_diagonal(q_ref[h])

    for d in range(3):
        v_from_y(d).wait_recv()
    for j in (1, 2):
        for copy in to_z(j, z):
            copy.start()

    def stage1(j):
        zs = slab(j)
        for copy in to_z(j, zs):
            copy.wait_recv()

        @pl.when(j <= 5)
        def _():
            for copy in to_z(j + 2, zs):
                copy.start()

        for d in range(3):
            k_to_y(j, d).start()

    def stage2(j):
        for d in range(3):
            k_from_y(j, d).wait_recv()
        for copy in to_sibling(j, c):
            copy.start()

    def stage3(j):
        for copy in to_sibling(j, 1 - c):
            copy.wait_recv()

    chip = z * NY + y
    lo = jnp.minimum(chip, 31 - chip)
    hi = 31 - lo

    ones = jnp.ones((16, KB), jnp.bfloat16)

    def keys(i):
        zs, yy = i // NY, lax.rem(i, NY)
        return jnp.concatenate([gk[zs, 0, yy], gk[zs, 1, yy]], axis=0)

    def values(i):
        zs, yy = i // NY, lax.rem(i, NY)
        v0, v1 = gv[zs, 0, yy], gv[zs, 1, yy]
        vt = jnp.concatenate([v0[:HALF], v0[HALF:], v1[:HALF], v1[HALF:]], axis=1)
        return jnp.concatenate([vt, ones], axis=0)

    def scores(i, t, slot, base=None):
        s = jnp.dot(keys(i), qbd[t], preferred_element_type=jnp.float32)
        if base is not None:
            key_pos = i * KB + lax.broadcasted_iota(jnp.int32, (KB, 2 * HALF), 0)
            row = lax.broadcasted_iota(jnp.int32, (KB, 2 * HALF), 1)
            row_pos = base + jnp.where(row < HALF, row, row - HALF)
            s = jnp.where(key_pos <= row_pos, s, NEG)
        sb[slot][...] = s
        bm[slot][...] = jnp.max(s, axis=0, keepdims=True)

    def weigh(i, t, slot):
        old = m_ref[t]
        new = jnp.maximum(old, bm[slot][...])
        m_ref[t] = new
        pb[slot][...] = jnp.exp(sb[slot][...] - new).astype(jnp.bfloat16)
        acc_ref[t] = acc_ref[t] * jnp.exp(old - new) + jnp.dot(
            values(i), pb[slot][...], preferred_element_type=jnp.float32
        )

    def sweep(begin, end, tiles):
        n = len(tiles)

        @pl.when(begin < end)
        def _():
            for u in range(LAG):
                scores(begin, tiles[u], u % NB)

            def step(i, carry):
                nxt = jnp.minimum(i + 1, end - 1)
                for u in range(n):
                    ahead = u + LAG
                    scores(i if ahead < n else nxt, tiles[ahead % n], ahead % NB)
                    weigh(i, tiles[u], u % NB)
                return carry

            lax.fori_loop(begin, end, step, 0)

    def masked(i, first, base):
        for u in range(LAG):
            scores(i, first + u, u % NB, base)
        for u in range(4):
            if u + LAG < 4:
                scores(i, first + u + LAG, (u + LAG) % NB, base)
            weigh(i, first + u, u % NB)

    p_own = me * ROWS
    p_far = partner["sp"] * ROWS + HALF
    base_lo = jnp.where(is_low, p_own, p_far)
    base_hi = jnp.where(is_low, p_far, p_own)

    def compute(j):
        zs = slab(j)
        first, last = zs * NY, zs * NY + NY
        sweep(first, jnp.minimum(last, lo), list(range(8)))
        sweep(jnp.maximum(first, lo), jnp.minimum(last, hi), list(range(4, 8)))
        in_lo = lo // NY == zs
        in_hi = hi // NY == zs

        def diagonal(g, carry):
            @pl.when(jnp.where(g == 0, in_lo, in_hi))
            def _():
                masked(jnp.where(g == 0, lo, hi), g * 4, jnp.where(g == 0, base_lo, base_hi))
            return carry

        lax.fori_loop(0, 2, diagonal, 0)

    stage1(1)
    stage2(0)
    q_copy.wait_recv()
    for h in range(4):
        qbd[g_far + h] = block_diagonal(qin[h])

    def per_slab(j, carry):
        @pl.when(j <= 5)
        def _():
            stage1(j + 2)

        @pl.when(j <= 6)
        def _():
            stage2(j + 1)

        stage3(j)
        compute(j)
        return carry

    lax.fori_loop(0, NZ, per_slab, 0)

    def finish(group, att_out, lse_out):
        for h in range(4):
            acc = acc_ref[group + h]
            m = m_ref[group + h]
            total = acc[HALF:HALF + 1]
            lse = m + jnp.log(total)
            lse_out[0, h:h + 1, :] = lse[:, :HALF]
            lse_out[1, h:h + 1, :] = lse[:, HALF:]
            both = acc[:HALF] / total
            out = both[:, :HALF] - lam_ref[h:h + 1, :] * both[:, HALF:]
            scale = lax.rsqrt(jnp.mean(out * out, axis=0, keepdims=True) + NORM_EPS)
            normed = out * scale * gain_ref[...]
            att_out[:, h * HALF:(h + 1) * HALF] = normed.T.astype(jnp.bfloat16)

    finish(g_far, attx, lsex)
    finish(g_own, att_ref.at[0], lse_ref.at[0])
    back = (remote(attx, attr, o_s.at[0], o_r.at[0], partner),
            remote(lsex, lser, o_s.at[1], o_r.at[1], partner))
    for copy in back:
        copy.start()

    q_copy.wait_send()
    for d in range(3):
        v_to_y(d).wait_send()

    def drain(j, carry):
        for d in range(3):
            k_to_y(j, d).wait_send()
        for copy in to_sibling(j, c):
            copy.wait_send()
        return carry

    lax.fori_loop(0, NZ, drain, 0)

    def drain_z(j, carry):
        for copy in to_z(j, z):
            copy.wait_send()
        return carry

    lax.fori_loop(1, NZ, drain_z, 0)
    for copy in back:
        copy.wait()
    att_ref[1] = attr[...]
    lse_ref[1] = lser[...]


def attend(queries, keys_own, values_own, lam, head_gain):
    qt = jnp.transpose(queries * jnp.asarray(0.125, jnp.bfloat16), (1, 2, 0))
    vt = values_own.reshape(2, HALF, 128).transpose(0, 2, 1).reshape(ROWS, 128)
    bf, f32 = jnp.bfloat16, jnp.float32
    dma = pltpu.SemaphoreType.DMA
    vmem = pl.BlockSpec(memory_space=pltpu.VMEM)
    return pl.pallas_call(
        attention_kernel,
        out_shape=(
            jax.ShapeDtypeStruct((2, HALF, 512), bf),
            jax.ShapeDtypeStruct((2, 2, 4, HALF), f32),
        ),
        in_specs=[vmem] * 6,
        out_specs=(vmem, vmem),
        scratch_shapes=[
            pltpu.VMEM((NZ, NC, NY, ROWS, 128), bf),
            pltpu.VMEM((NZ, NC, NY, ROWS, 128), bf),
            pltpu.VMEM((8, 128, 256), bf),
            pltpu.VMEM((4, 128, 128), bf),
            pltpu.VMEM((8, 1, 256), f32),
            pltpu.VMEM((8, 144, 256), f32),
            pltpu.VMEM((HALF, 512), bf),
            pltpu.VMEM((2, 4, HALF), f32),
            pltpu.VMEM((HALF, 512), bf),
            pltpu.VMEM((2, 4, HALF), f32),
            *[pltpu.VMEM((KB, 256), f32)] * NB,
            *[pltpu.VMEM((KB, 256), bf)] * NB,
            *[pltpu.VMEM((1, 256), f32)] * NB,
            dma((2,)),
            dma((8, 3)), dma((8, 3)), dma((3,)), dma((3,)),
            dma((8,)), dma((8,)), dma((8,)), dma((8,)),
            dma((8,)), dma((8,)), dma((8,)), dma((8,)),
            dma, dma, dma((2,)), dma((2,)),
        ],
        compiler_params=pltpu.CompilerParams(
            collective_id=0, has_side_effects=True, vmem_limit_bytes=48 * 2**20
        ),
        name="attend",
    )(
        qt[:, :, :HALF], qt[:, :, HALF:], keys_own, vt,
        jnp.broadcast_to(lam[:, None], (4, HALF)),
        jnp.broadcast_to(head_gain[:, None], (128, HALF)),
    )


def local(
    tokens,
    norm_gain,
    query_weight,
    key_weight,
    value_weight,
    mix_lambda,
    head_gain,
    pool_weight,
    pool_mix,
    pool_scale,
    gate_weight,
    out_weight,
):
    model_width = tokens.shape[1]
    heads_local = query_weight.shape[1]
    group_width = pool_weight.shape[2]
    channels = gate_weight.shape[2]
    matrices = (
        query_weight.reshape(model_width, -1),
        key_weight.reshape(model_width, -1),
        value_weight.reshape(model_width, -1),
        pool_weight.reshape(model_width, -1),
        gate_weight.reshape(model_width, -1),
    )
    rows = copy_for_each(tokens, "tp").reshape(-1, model_width)
    inputs = rows.astype(jnp.float32)
    normed = (
        inputs
        * lax.rsqrt(jnp.mean(inputs * inputs, axis=1, keepdims=True) + NORM_EPS)
        * norm_gain
    ).astype(jnp.bfloat16)
    queries, keys_own, values_own, pool_in, gate_pre = [
        jnp.dot(normed, matrix, preferred_element_type=jnp.float32).astype(jnp.bfloat16)
        for matrix in matrices
    ]
    tok_rows = rows.shape[0]
    rim_prev = shifted(pool_in[tok_rows - WINDOW :], "sp", 1)
    att, lse = attend(
        queries.reshape(tok_rows, heads_local, 128), keys_own, values_own, mix_lambda, head_gain
    )
    attended = att.reshape(tok_rows, 512).astype(jnp.float32)
    log_out = jnp.concatenate([lse[0], lse[1]], axis=2)
    gate_pre = gate_pre.reshape(tok_rows, 2, channels)
    positions = lax.axis_index("sp") * tok_rows + jnp.arange(tok_rows, dtype=jnp.int32)
    extended = jnp.concatenate([rim_prev, pool_in], axis=0).astype(jnp.float32)
    window_span = jnp.left_shift(jnp.int32(2), lax.axis_index("tp"))
    window_sum = jnp.zeros((tok_rows, group_width), jnp.float32)
    for back_rows in range(WINDOW):
        window_sum = window_sum + jnp.where(
            back_rows < window_span,
            extended[WINDOW - back_rows : WINDOW - back_rows + tok_rows],
            0.0,
        )
    counts = jnp.minimum(positions + 1, window_span).astype(jnp.float32)
    means = window_sum / counts[:, None]
    pooled = (means - pool_in.astype(jnp.float32)).astype(jnp.bfloat16)
    group_parts = jnp.dot(pooled, pool_mix[0], preferred_element_type=jnp.float32) * pool_scale[0]
    merged = (
        jax.nn.sigmoid(gate_pre[:, 0].astype(jnp.float32)) * attended
        + jax.nn.sigmoid(gate_pre[:, 1].astype(jnp.float32)) * group_parts
    ).astype(jnp.bfloat16)
    mixed = sent_and_summed(
        jnp.dot(merged, out_weight, preferred_element_type=jnp.float32).astype(jnp.bfloat16),
        "tp",
    )
    return (mixed.astype(jnp.bfloat16), log_out)


def solution(mesh):
    in_specs = (
        P(("sp", "tp"), None),
        P(),
        P(None, "tp", None),
        P(None, "tp", None),
        P(None, "tp", None),
        P("tp"),
        P(),
        P(None, "tp", None),
        P("tp", None, None),
        P("tp", None),
        P(None, None, "tp"),
        P("tp", None),
    )
    out_specs = (P(("sp", "tp"), None), P(None, "tp", "sp"))
    return jax.shard_map(local, mesh=mesh, in_specs=in_specs, out_specs=out_specs, check_vma=False)
```

time: 332 us -> 147 us (0.44)
  the two profiles are of different devices: /device:TPU:248 before, /device:TPU:96 now
where the time goes in v1:
time: 147 us; the launch traced here: 146 us
  Pallas kernels  80.2 us (55%)
  waiting for transfers between devices  24.8 us (17%)
  local copies, waits for them, and re-layouts  14.6 us (10%)
  matrix products  12.8 us (9%)
  starting transfers between devices  9.9 us (7%)
  other arithmetic  3.14 us (2%)
    pallas_call x1, Pallas kernels, attend(): pl.pallas_call(attention_kernel, out_shape=(jax.ShapeDtypeStruct((2, HALF...  80.2 us
    all_to_all x1, waiting for transfers between devices, sent_and_summed(): lax.all_to_all(array.reshape(size, -1, array.shape[1]), axis, 0, 0, tiled...  15 us
    all_to_all x1, waiting for transfers between devices, copy_for_each(): lax.all_to_all(jnp.broadcast_to(array[None], (size, *array.shape)), axis,...  9.75 us
    dot_general x5, matrix products, local(): jnp.dot(normed, matrix, preferred_element_type=jnp.float32)  8.4 us
    unnamed x23, local copies, waits for them, and re-layouts  7.05 us
    dot_general x1, matrix products, local(): jnp.dot(merged, out_weight, preferred_element_type=jnp.float32)  4.36 us
    all_to_all x1, starting transfers between devices, copy_for_each(): lax.all_to_all(jnp.broadcast_to(array[None], (size, *array.shape)), axis,...  4.29 us
    all_to_all x1, starting transfers between devices, sent_and_summed(): lax.all_to_all(array.reshape(size, -1, array.shape[1]), axis, 0, 0, tiled...  3.51 us
  transfers between devices with their start and end apart: 3, of which 2 were waited for; matrix products, arithmetic and copies ran while one was open for 8% of the time, Pallas kernels for 55%

profile of v1, /device:TPU:96, one launch (start us, length us, event | category | flops | bytes accessed | tf_op | source)
XLA Modules:
  0.0 146.1 jit_solution(12402265034552286153)
XLA Ops:
  0.6 0.0 copy-start
  0.6 2.2 %broadcast_in_dim.40 = bf16[4,64,2048]{2,1,0:T(8,128)(2,1)} broadcast(bf16[64,2048]{1,0:T(8,128)(2,1)} %param.12), dimensions={1,2} | broadcast | bytes 1310720 | tf_op jit(solution)/shard_map/broadcast_in_dim | solution.py:24
  2.8 4.3 %all-to-all-start = ((bf16[4,64,2048]{2,1,0:T(8,128)(2,1)}), bf16[4,64,2048]{2,1,0:T(8,128)(2,1)S(1)}, u32[]{:S(2)}, u32[]{:S(2)}) async-start(bf16[4,64,2048]{2,1,0:T(8,128)(2,1)} %broadcast_in_dim.40), calls=%async_computation | async-start | bytes 2097152 | tf_op jit(solution)/shard_map/all_to_all | solution.py:23
  7.1 5.3 %copy.24 = bf16[256,8,2,512]{3,1,2,0:T(8,128)(2,1)} copy(bf16[256,8,2,512]{3,2,1,0:T(2,128)(2,1)} %bitcast.65) | data formatting | bytes 8388608
  12.5 9.7 %all-to-all-done = bf16[4,64,2048]{2,1,0:T(8,128)(2,1)S(1)} async-done(((bf16[4,64,2048]{2,1,0:T(8,128)(2,1)}), bf16[4,64,2048]{2,1,0:T(8,128)(2,1)S(1)}, u32[]{:S(2)}, u32[]{:S(2)}) %all-to-all-start) | async-done | bytes 1048608 | tf_op jit(solution)/shard_map/all_to_all | solution.py:23
  22.2 0.3 fusion
  22.5 0.3 fusion.2
  22.9 1.0 copy-done.1
  23.8 1.4 fusion.17
  25.3 1.2 copy.19
  26.4 0.0 copy-start.9
  26.5 1.9 %convolution_convert_fusion.3.k_ref = bf16[256,128]{1,0:T(8,128)(2,1)S(1)} fusion(bf16[256,2048]{1,0:T(8,128)(2,1)} %bitcast.61, bf16[2048,1,128]{2,0,1:T(8,128)(2,1)} %param.15), kind=kOutput, calls=%fused_computation.20 | convolution fusion | flops 134250496 | bytes 1638400 | tf_op jit(solution)/shard_map/dot_general | solution.py:388
  28.4 2.2 %convolution_convert_fusion.2 = bf16[256,128]{1,0:T(8,128)(2,1)} fusion(bf16[256,2048]{1,0:T(8,128)(2,1)S(1)} %bitcast.62, bf16[2048,1,128]{2,0,1:T(8,128)(2,1)} %param.16), kind=kOutput, calls=%fused_computation.19 | convolution fusion | flops 134250496 | bytes 1638400 | tf_op jit(solution)/shard_map/dot_general | solution.py:388
  30.7 0.7 fusion.11
  31.4 0.0 copy-start.4
  31.4 0.7 copy-done.4
  32.1 2.1 %collective-permute-start = (bf16[16,512]{1,0:T(8,128)(2,1)S(1)}, bf16[16,512]{1,0:T(8,128)(2,1)S(1)}, u32[]{:S(2)}, u32[]{:S(2)}) collective-permute-start(bf16[16,512]{1,0:T(8,128)(2,1)S(1)} %slice.96), channel_id=1, source_target_pairs={{0,4},{4,8},{8,12},{12,16},{16,20},{20,24},{24,28},{28,32},{32,36}... | collective-permute-start | bytes 49160 | tf_op jit(solution)/shard_map/ppermute | solution.py:31
  34.2 2.1 %convolution_convert_fusion.1 = bf16[256,1024]{1,0:T(8,128)(2,1)} fusion(bf16[256,2048]{1,0:T(8,128)(2,1)S(1)} %bitcast.64, bf16[2048,1024]{1,0:T(8,128)(2,1)S(1)} %bitcast.66), kind=kOutput, calls=%fused_computation.11 | convolution fusion | flops 1074003968 | bytes 5767168 | tf_op jit(solution)/shard_map/dot_general | solution.py:388
  36.3 1.5 reshape.122
  37.7 0.0 copy-start.10
  37.7 1.6 %fusion.99 = (bf16[256,1,512]{2,1,0:T(2,128)(2,1)S(1)}, bf16[256,1,512]{2,1,0:T(2,128)(2,1)}) fusion(bf16[256,2,512]{2,1,0:T(2,128)(2,1)S(1)} %reshape.122), kind=kLoop, calls=%fused_computation.101 | loop fusion | bytes 1048576 | tf_op jit(solution)/shard_map/slice | solution.py:414
  39.4 0.9 copy.20
  40.3 0.1 broadcast_in_dim.41.lam_ref
  40.4 0.1 broadcast_in_dim.42.gain_ref
  40.5 80.2 %attend.1 = (bf16[2,128,512]{2,1,0:T(8,128)(2,1)S(1)}, f32[2,2,4,128]{3,2,1,0:T(4,128)S(1)}) custom-call(bf16[4,128,128]{2,1,0:T(8,128)(2,1)S(1)} %get-tuple-element.9.q_ref, bf16[4,128,128]{2,1,0:T(8,128)(2,1)S(1)} %get-tuple-element.8.qs_ref, bf16[256,128]{1,0:T(8,128)(2,1)S(1)} %convolution_convert_fusion.3.k_ref, bf16[256,128]{1,0:T(8,128)(2,1)S(1)} %bitcast.58, ...), custom_call_target="tpu_custom_call" | custom-call | tf_op jit(solution)/shard_map/attend/pallas_call | solution.py:316
  120.7 0.0 collective-permute-done
  120.7 1.0 maximum_convert_fusion
  121.7 4.4 %convolution_convert_fusion = bf16[256,2048]{1,0:T(8,128)(2,1)} fusion(bf16[512,2048]{1,0:T(8,128)(2,1)S(1)} %copy-done, bf16[256,512]{1,0:T(8,128)(2,1)S(1)} %bitcast.59, bf16[1,512,512]{2,1,0:T(8,128)(2,1)} %param.20, bf16[256,512]{1,0:T(8,128)(2,1)} %copy-done.4, f32[272,512]{1,0:T(8,128)S(1)} %maximum_convert_fusion, ...), kind=kOutput, calls=%fused_computation.2 | convolution fusion | flops 678035456 | bytes 13372432 | tf_op jit(solution)/shard_map/dot_general | solution.py:418
  126.1 3.5 %all-to-all-start.1 = ((bf16[4,64,2048]{2,1,0:T(8,128)(2,1)}), bf16[4,64,2048]{2,1,0:T(8,128)(2,1)S(1)}, u32[]{:S(2)}, u32[]{:S(2)}) async-start(bf16[4,64,2048]{2,1,0:T(8,128)(2,1)} %bitcast.67), calls=%async_computation.1 | async-start | bytes 2097152 | tf_op jit(solution)/shard_map/all_to_all | solution.py:36
  129.6 0.6 pad_maximum_fusion
  130.2 15.0 %all-to-all-done.1 = bf16[4,64,2048]{2,1,0:T(8,128)(2,1)S(1)} async-done(((bf16[4,64,2048]{2,1,0:T(8,128)(2,1)}), bf16[4,64,2048]{2,1,0:T(8,128)(2,1)S(1)}, u32[]{:S(2)}, u32[]{:S(2)}) %all-to-all-start.1) | async-done | bytes 1048608 | tf_op jit(solution)/shard_map/all_to_all | solution.py:36
  145.2 0.9 reduce_sum.22
  (21 shorter events, 0.1 us)
Async XLA Ops:
  0.6 121.1 %copy-start = (bf16[512,2048]{1,0:T(8,128)(2,1)S(1)}, bf16[512,2048]{1,0:T(8,128)(2,1)}, u32[]{:S(2)}) copy-start(bf16[512,2048]{1,0:T(8,128)(2,1)} %param.23) | copy-start | bytes 6291460
  2.8 19.4 %all-to-all-start = ((bf16[4,64,2048]{2,1,0:T(8,128)(2,1)}), bf16[4,64,2048]{2,1,0:T(8,128)(2,1)S(1)}, u32[]{:S(2)}, u32[]{:S(2)}) async-start(bf16[4,64,2048]{2,1,0:T(8,128)(2,1)} %broadcast_in_dim.40), calls=%async_computation | async-start | bytes 2097152 | tf_op jit(solution)/shard_map/all_to_all | solution.py:23
  7.1 15.4 %copy-start.5 = (f32[2048]{0:T(1024)S(1)}, f32[2048]{0:T(1024)}, u32[]{:S(2)}) copy-start(f32[2048]{0:T(1024)} %param.13) | copy-start | bytes 24580
  22.2 1.6 %copy-start.8 = (bf16[2048,4,128]{2,1,0:T(4,128)(2,1)S(1)}, bf16[2048,4,128]{2,1,0:T(4,128)(2,1)}, u32[]{:S(2)}) copy-start(bf16[2048,4,128]{2,1,0:T(4,128)(2,1)} %param.14) | copy-start | bytes 6291460
  22.8 1.0 copy-start.1
  25.3 3.1 %copy-start.2 = (bf16[4,64,2048]{2,1,0:T(8,128)(2,1)S(1)}, bf16[4,64,2048]{2,1,0:T(8,128)(2,1)}, u32[]{:S(2)}) copy-start(bf16[4,64,2048]{2,1,0:T(8,128)(2,1)} %copy-done.1) | copy-start | bytes 3145732
  26.4 4.2 %copy-start.9 = (bf16[2048,1,512]{2,0,1:T(8,128)(2,1)S(1)}, bf16[2048,1,512]{2,0,1:T(8,128)(2,1)}, u32[]{:S(2)}) copy-start(bf16[2048,1,512]{2,0,1:T(8,128)(2,1)} %param.19) | copy-start | bytes 6291460
  28.4 5.8 %copy-start.3 = (bf16[256,8,2,512]{3,1,2,0:T(8,128)(2,1)S(1)}, bf16[256,8,2,512]{3,1,2,0:T(8,128)(2,1)}, u32[]{:S(2)}) copy-start(bf16[256,8,2,512]{3,1,2,0:T(8,128)(2,1)} %copy.24) | copy-start | bytes 12582916
  31.4 0.7 copy-start.4
  32.1 88.6 %collective-permute-start = (bf16[16,512]{1,0:T(8,128)(2,1)S(1)}, bf16[16,512]{1,0:T(8,128)(2,1)S(1)}, u32[]{:S(2)}, u32[]{:S(2)}) collective-permute-start(bf16[16,512]{1,0:T(8,128)(2,1)S(1)} %slice.96), channel_id=1, source_target_pairs={{0,4},{4,8},{8,12},{12,16},{16,20},{20,24},{24,28},{28,32},{32,36}... | collective-permute-start | bytes 49160 | tf_op jit(solution)/shard_map/ppermute | solution.py:31
  36.3 4.0 %copy-start.7 = (f32[4]{0:T(128)S(1)}, f32[4]{0:T(128)}, u32[]{:S(2)}) copy-start(f32[4]{0:T(128)} %param.17) | copy-start | bytes 52
  36.3 4.1 %copy-start.6 = (f32[128]{0:T(128)S(1)}, f32[128]{0:T(128)}, u32[]{:S(2)}) copy-start(f32[128]{0:T(128)} %param.18) | copy-start | bytes 1540
  37.7 84.0 %copy-start.10 = (f32[1,512]{1,0:T(1,128)S(1)}, f32[1,512]{1,0:T(1,128)}, u32[]{:S(2)}) copy-start(f32[1,512]{1,0:T(1,128)} %param.21) | copy-start | bytes 6148
  126.1 19.2 %all-to-all-start.1 = ((bf16[4,64,2048]{2,1,0:T(8,128)(2,1)}), bf16[4,64,2048]{2,1,0:T(8,128)(2,1)S(1)}, u32[]{:S(2)}, u32[]{:S(2)}) async-start(bf16[4,64,2048]{2,1,0:T(8,128)(2,1)} %bitcast.67), calls=%async_computation.1 | async-start | bytes 2097152 | tf_op jit(solution)/shard_map/all_to_all | solution.py:36

commit v2 on v1

--- a/solution.py
+++ b/solution.py
@@ -12,10 +12,10 @@
 MESH = pl.DeviceIdType.MESH
 NEG = -1e30
 NZ, NY, NC = 8, 4, 2
-LAG, NB = 2, 4
+LAG, NB = 3, 4
 ROWS = 256
 HALF = 128
-KB = 512
+KB = 1024
 
 
 def copy_for_each(array, axis):
@@ -40,12 +40,12 @@
 def attention_kernel(
     q_ref, qs_ref, k_ref, v_ref, lam_ref, gain_ref,
     att_ref, lse_ref,
-    gk, gv, qbd, qin, m_ref, acc_ref, attx, lsex, attr, lser,
+    kv, qbd, qin, m_ref, acc_ref, attx, lsex, attr, lser,
     *rest,
 ):
     sb, pb, bm = rest[:NB], rest[NB:2 * NB], rest[2 * NB:3 * NB]
-    (own_sem, ky_s, ky_r, vy_s, vy_r, kz_s, kz_r, vz_s, vz_r,
-     sk_s, sk_r, sv_s, sv_r, q_s, q_r, o_s, o_r) = rest[3 * NB:]
+    (own_sem, y_s, y_r, vy_s, vy_r, z_s, z_r,
+     sib_s, sib_r, q_s, q_r, o_s, o_r) = rest[3 * NB:]
     me = lax.axis_index("sp")
     z, y, c = me // (NY * NC), (me // NC) % NY, me % NC
 
@@ -54,11 +54,11 @@
 
     sibling = at(z, y, 1 - c)
     partner = at(NZ - 1 - z, NY - 1 - y, c)
-    z_up, z_down = at((z + 1) % NZ, y, c), at((z + NZ - 1) % NZ, y, c)
+    z_next = [at((z + 1) % NZ, y, c), at((z + NZ - 1) % NZ, y, c)]
     y_peers = [at(z, (y + d) % NY, c) for d in (1, 2, 3)]
 
     barrier = pltpu.get_barrier_semaphore()
-    peers = [sibling, partner, z_up, z_down, *y_peers]
+    peers = [sibling, partner, *z_next, *y_peers]
     for peer in peers:
         pl.semaphore_signal(barrier, inc=1, device_id=peer, device_id_type=MESH)
     pl.semaphore_wait(barrier, len(peers))
@@ -69,50 +69,53 @@
             device_id=dev, device_id_type=MESH,
         )
 
-    def slab(j):
-        k = (j + 1) // 2
-        return lax.rem(z + NZ + jnp.where(lax.rem(j, 2) == 1, -k, k), NZ)
-
-    def k_to_y(j, d):
-        zs = slab(j)
-        return remote(gk.at[zs, c, y], gk.at[zs, c, y], ky_s.at[j, d], ky_r.at[j, d], y_peers[d])
-
-    def k_from_y(j, d):
-        zs, yy = slab(j), lax.rem(y + NY - (d + 1), NY)
-        return remote(gk.at[zs, c, yy], gk.at[zs, c, yy], ky_s.at[j, d], ky_r.at[j, d], y_peers[d])
+    def slab(k, way):
+        return lax.rem(z + NZ + (k if way else -k), NZ)
+
+    def k_to_y(k, way, d):
+        piece = kv.at[slab(k, way), c, 0, y]
+        return remote(piece, piece, y_s.at[way, k, d], y_r.at[way, k, d], y_peers[d])
+
+    def k_from_y(k, way, d):
+        piece = kv.at[slab(k, way), c, 0, lax.rem(y + NY - (d + 1), NY)]
+        return remote(piece, piece, y_s.at[way, k, d], y_r.at[way, k, d], y_peers[d])
 
     def v_to_y(d):
-        return remote(v_ref, gv.at[z, c, y], vy_s.at[d], vy_r.at[d], y_peers[d])
+        return remote(v_ref, kv.at[z, c, 1, y], vy_s.at[d], vy_r.at[d], y_peers[d])
 
     def v_from_y(d):
         yy = lax.rem(y + NY - (d + 1), NY)
-        return remote(v_ref, gv.at[z, c, yy], vy_s.at[d], vy_r.at[d], y_peers[d])
-
-    def to_z(j, zs):
-        dev = {"sp": jnp.where(lax.rem(j, 2) == 1, z_up["sp"], z_down["sp"])}
-        return (
-            remote(gk.at[zs, c, y], gk.at[zs, c, y], kz_s.at[j], kz_r.at[j], dev),
-            remote(gv.at[zs, c], gv.at[zs, c], vz_s.at[j], vz_r.at[j], dev),
+        return remote(v_ref, kv.at[z, c, 1, yy], vy_s.at[d], vy_r.at[d], y_peers[d])
+
+    def z_piece(zs, r):
+        kind = jnp.minimum(r, 1)
+        return kv.at[zs, c, kind, lax.rem(y + jnp.maximum(r - 1, 0), NY)]
+
+    def z_msg(k, r, way, src_k, src=None):
+        piece = z_piece(slab(src_k, way), r)
+        return remote(
+            piece if src is None else src, piece,
+            z_s.at[way, k, r], z_r.at[way, k, r], z_next[way],
         )
 
-    def to_sibling(j, cc):
-        zs = slab(j)
-        return (
-            remote(gk.at[zs, cc], gk.at[zs, cc], sk_s.at[j], sk_r.at[j], sibling),
-            remote(gv.at[zs, cc], gv.at[zs, cc], sv_s.at[j], sv_r.at[j], sibling),
-        )
-
+    def to_sibling(k, way, cc):
+        part = kv.at[slab(k, way), cc]
+        return remote(part, part, sib_s.at[way, k], sib_r.at[way, k], sibling)
+
+    own_k = pltpu.make_async_copy(k_ref, kv.at[z, c, 0, y], own_sem.at[0])
+    own_v = pltpu.make_async_copy(v_ref, kv.at[z, c, 1, y], own_sem.at[1])
+    own_k.start()
+    own_v.start()
+    for d in (0, 2, 1):
+        v_to_y(d).start()
+    for way in (0, 1):
+        z_msg(1, 0, way, 0, k_ref).start()
+        z_msg(1, 1, way, 0, v_ref).start()
     q_copy = remote(qs_ref, qin, q_s, q_r, partner)
     q_copy.start()
-    own_k = pltpu.make_async_copy(k_ref, gk.at[z, c, y], own_sem.at[0])
-    own_v = pltpu.make_async_copy(v_ref, gv.at[z, c, y], own_sem.at[1])
-    own_k.start()
-    own_v.start()
-    for d in range(3):
-        v_to_y(d).start()
     own_k.wait()
-    for d in range(3):
-        k_to_y(0, d).start()
+    for d in (0, 2, 1):
+        k_to_y(0, 0, d).start()
     own_v.wait()
 
     m_ref[...] = jnp.full_like(m_ref, NEG)
@@ -129,50 +132,27 @@
     for h in range(4):
         qbd[g_own + h] = block_diagonal(q_ref[h])
 
-    for d in range(3):
-        v_from_y(d).wait_recv()
-    for j in (1, 2):
-        for copy in to_z(j, z):
-            copy.start()
-
-    def stage1(j):
-        zs = slab(j)
-        for copy in to_z(j, zs):
-            copy.wait_recv()
-
-        @pl.when(j <= 5)
-        def _():
-            for copy in to_z(j + 2, zs):
-                copy.start()
-
-        for d in range(3):
-            k_to_y(j, d).start()
-
-    def stage2(j):
-        for d in range(3):
-            k_from_y(j, d).wait_recv()
-        for copy in to_sibling(j, c):
-            copy.start()
-
-    def stage3(j):
-        for copy in to_sibling(j, 1 - c):
-            copy.wait_recv()
-
-    chip = z * NY + y
-    lo = jnp.minimum(chip, 31 - chip)
-    hi = 31 - lo
+    for r in (2, 4, 3):
+        v_from_y(NY - r).wait_recv()
+        for way in (0, 1):
+            z_msg(1, r, way, 0).start()
+
+    mine = (z * NY + y) // 2
+    lo = jnp.minimum(mine, 15 - mine)
+    hi = 15 - lo
 
     ones = jnp.ones((16, KB), jnp.bfloat16)
 
+    def pieces(i, kind):
+        zs, yy = i // 2, 2 * lax.rem(i, 2)
+        return [kv[zs, cc, kind, yy + d] for d in (0, 1) for cc in (0, 1)]
+
     def keys(i):
-        zs, yy = i // NY, lax.rem(i, NY)
-        return jnp.concatenate([gk[zs, 0, yy], gk[zs, 1, yy]], axis=0)
+        return jnp.concatenate(pieces(i, 0), axis=0)
 
     def values(i):
-        zs, yy = i // NY, lax.rem(i, NY)
-        v0, v1 = gv[zs, 0, yy], gv[zs, 1, yy]
-        vt = jnp.concatenate([v0[:HALF], v0[HALF:], v1[:HALF], v1[HALF:]], axis=1)
-        return jnp.concatenate([vt, ones], axis=0)
+        halves = [v[a:a + HALF] for v in pieces(i, 1) for a in (0, HALF)]
+        return jnp.concatenate([jnp.concatenate(halves, axis=1), ones], axis=0)
 
     def scores(i, t, slot, base=None):
         s = jnp.dot(keys(i), qbd[t], preferred_element_type=jnp.float32)
@@ -193,73 +173,112 @@
             values(i), pb[slot][...], preferred_element_type=jnp.float32
         )
 
-    def sweep(begin, end, tiles):
+    def block(i, tiles, base=None):
         n = len(tiles)
-
-        @pl.when(begin < end)
-        def _():
-            for u in range(LAG):
-                scores(begin, tiles[u], u % NB)
-
-            def step(i, carry):
-                nxt = jnp.minimum(i + 1, end - 1)
-                for u in range(n):
-                    ahead = u + LAG
-                    scores(i if ahead < n else nxt, tiles[ahead % n], ahead % NB)
-                    weigh(i, tiles[u], u % NB)
-                return carry
-
-            lax.fori_loop(begin, end, step, 0)
-
-    def masked(i, first, base):
         for u in range(LAG):
-            scores(i, first + u, u % NB, base)
-        for u in range(4):
-            if u + LAG < 4:
-                scores(i, first + u + LAG, (u + LAG) % NB, base)
-            weigh(i, first + u, u % NB)
+            scores(i, tiles[u], u % NB, base)
+        for u in range(n):
+            if u + LAG < n:
+                scores(i, tiles[u + LAG], (u + LAG) % NB, base)
+            weigh(i, tiles[u], u % NB)
 
     p_own = me * ROWS
     p_far = partner["sp"] * ROWS + HALF
     base_lo = jnp.where(is_low, p_own, p_far)
     base_hi = jnp.where(is_low, p_far, p_own)
 
-    def compute(j):
-        zs = slab(j)
-        first, last = zs * NY, zs * NY + NY
-        sweep(first, jnp.minimum(last, lo), list(range(8)))
-        sweep(jnp.maximum(first, lo), jnp.minimum(last, hi), list(range(4, 8)))
-        in_lo = lo // NY == zs
-        in_hi = hi // NY == zs
-
-        def diagonal(g, carry):
-            @pl.when(jnp.where(g == 0, in_lo, in_hi))
+    def compute(i):
+        @pl.when(i < lo)
+        def _():
+            block(i, list(range(8)))
+
+        @pl.when((i >= lo) & (i < hi))
+        def _():
+            block(i, list(range(4, 8)))
+
+        @pl.when((i == lo) | (i == hi))
+        def _():
+            first = jnp.where(i == lo, 0, 4)
+            block(i, [first + u for u in range(4)], jnp.where(i == lo, base_lo, base_hi))
+
+    def share(k, ways):
+        for way in ways:
+            for d in range(3):
+                k_from_y(k, way, d).wait_recv()
+            to_sibling(k, way, c).start()
+
+    def shared(k, ways):
+        for way in ways:
+            to_sibling(k, way, 1 - c).wait_recv()
+
+    def serve(k, r, way, forward):
+        z_msg(k, r, way, k).wait_recv()
+        if forward is not None:
+            @pl.when(forward)
             def _():
-                masked(jnp.where(g == 0, lo, hi), g * 4, jnp.where(g == 0, base_lo, base_hi))
-            return carry
-
-        lax.fori_loop(0, 2, diagonal, 0)
-
-    stage1(1)
-    stage2(0)
-    q_copy.wait_recv()
-    for h in range(4):
-        qbd[g_far + h] = block_diagonal(qin[h])
-
-    def per_slab(j, carry):
-        @pl.when(j <= 5)
-        def _():
-            stage1(j + 2)
-
-        @pl.when(j <= 6)
-        def _():
-            stage2(j + 1)
-
-        stage3(j)
-        compute(j)
+                z_msg(k + 1, r, way, k).start()
+
+        @pl.when(r == 0)
+        def _():
+            for d in (0, 2, 1):
+                k_to_y(k, way, d).start()
+
+    def both(k, r):
+        serve(k, r, 0, (k < 3) | (r <= 2))
+        serve(k, r, 1, (k < 3) | (r >= 3))
+
+    def tick(n, carry):
+        k, r = n // 5 + 1, lax.rem(n, 5)
+
+        @pl.when(k <= 3)
+        def _():
+            both(k, r)
+
+        @pl.when((k == 4) & (r <= 2))
+        def _():
+            serve(k, r, 0, None)
+
+        @pl.when((k == 4) & (r <= 1))
+        def _():
+            z_msg(k, r + 3, 1, k).wait_recv()
+
+        @pl.when((r == 4) & (k <= 3))
+        def _():
+            share(k, (0, 1))
+
+        @pl.when(r == 1)
+        def _():
+            shared(k - 1, (0,))
+
+            @pl.when(k > 1)
+            def _():
+                shared(k - 1, (1,))
+
+            @pl.when(k == 1)
+            def _():
+                q_copy.wait_recv()
+                for h in range(4):
+                    qbd[g_far + h] = block_diagonal(qin[h])
+
+        way = lax.rem(r + 1, 2)
+        far = lax.rem(z + NZ + jnp.where(way == 0, 1 - k, k - 1), NZ)
+
+        @pl.when((r >= 1) & ((way == 0) | (k > 1)))
+        def _():
+            compute(far * 2 + (r - 1) // 2)
+
         return carry
 
-    lax.fori_loop(0, NZ, per_slab, 0)
+    share(0, (0,))
+    lax.fori_loop(0, 20, tick, 0)
+    share(4, (0,))
+    shared(4, (0,))
+
+    def last(yy, carry):
+        compute(slab(4, 0) * 2 + yy)
+        return carry
+
+    lax.fori_loop(0, 2, last, 0)
 
     def finish(group, att_out, lse_out):
         for h in range(4):
@@ -269,8 +288,8 @@
             lse = m + jnp.log(total)
             lse_out[0, h:h + 1, :] = lse[:, :HALF]
             lse_out[1, h:h + 1, :] = lse[:, HALF:]
-            both = acc[:HALF] / total
-            out = both[:, :HALF] - lam_ref[h:h + 1, :] * both[:, HALF:]
+            ratio = acc[:HALF] / total
+            out = ratio[:, :HALF] - lam_ref[h:h + 1, :] * ratio[:, HALF:]
             scale = lax.rsqrt(jnp.mean(out * out, axis=0, keepdims=True) + NORM_EPS)
             normed = out * scale * gain_ref[...]
             att_out[:, h * HALF:(h + 1) * HALF] = normed.T.astype(jnp.bfloat16)
@@ -285,22 +304,24 @@
     q_copy.wait_send()
     for d in range(3):
         v_to_y(d).wait_send()
-
-    def drain(j, carry):
-        for d in range(3):
-            k_to_y(j, d).wait_send()
-        for copy in to_sibling(j, c):
-            copy.wait_send()
+        k_to_y(0, 0, d).wait_send()
+    to_sibling(0, 0, c).wait_send()
+
+    def drain(k, carry):
+        for way in (0, 1):
+            for r in range(5):
+                z_msg(k, r, way, 0).wait_send()
+            for d in range(3):
+                k_to_y(k, way, d).wait_send()
+            to_sibling(k, way, c).wait_send()
         return carry
 
-    lax.fori_loop(0, NZ, drain, 0)
-
-    def drain_z(j, carry):
-        for copy in to_z(j, z):
-            copy.wait_send()
-        return carry
-
-    lax.fori_loop(1, NZ, drain_z, 0)
+    lax.fori_loop(1, 4, drain, 0)
+    for r in range(5):
+        z_msg(4, r, 0 if r <= 2 else 1, 0).wait_send()
+    for d in range(3):
+        k_to_y(4, 0, d).wait_send()
+    to_sibling(4, 0, c).wait_send()
     for copy in back:
         copy.wait()
     att_ref[1] = attr[...]
@@ -322,8 +343,7 @@
         in_specs=[vmem] * 6,
         out_specs=(vmem, vmem),
         scratch_shapes=[
-            pltpu.VMEM((NZ, NC, NY, ROWS, 128), bf),
-            pltpu.VMEM((NZ, NC, NY, ROWS, 128), bf),
+            pltpu.VMEM((NZ, NC, 2, NY, ROWS, 128), bf),
             pltpu.VMEM((8, 128, 256), bf),
             pltpu.VMEM((4, 128, 128), bf),
             pltpu.VMEM((8, 1, 256), f32),
@@ -336,9 +356,8 @@
             *[pltpu.VMEM((KB, 256), bf)] * NB,
             *[pltpu.VMEM((1, 256), f32)] * NB,
             dma((2,)),
-            dma((8, 3)), dma((8, 3)), dma((3,)), dma((3,)),
-            dma((8,)), dma((8,)), dma((8,)), dma((8,)),
-            dma((8,)), dma((8,)), dma((8,)), dma((8,)),
+            dma((2, 5, 3)), dma((2, 5, 3)), dma((3,)), dma((3,)),
+            dma((2, 5, 5)), dma((2, 5, 5)), dma((2, 5)), dma((2, 5)),
             dma, dma, dma((2,)), dma((2,)),
         ],
         compiler_params=pltpu.CompilerParams(

time: 147 us -> 138 us (0.939)
  the two profiles are of different devices: /device:TPU:96 before, /device:TPU:1 now
where the time goes in v2:
time: 138 us; the launch traced here: 137 us
  Pallas kernels  69.6 us (50%)
  waiting for transfers between devices  22.1 us (16%)
  local copies, waits for them, and re-layouts  14.6 us (11%)
  starting transfers between devices  14.1 us (10%)
  matrix products  12.8 us (9%)
  other arithmetic  3.14 us (2%)
    pallas_call x1, Pallas kernels, attend(): pl.pallas_call(attention_kernel, out_shape=(jax.ShapeDtypeStruct((2, HALF...  69.6 us
    all_to_all x1, waiting for transfers between devices, sent_and_summed(): lax.all_to_all(array.reshape(size, -1, array.shape[1]), axis, 0, 0, tiled...  14.1 us
    dot_general x5, matrix products, local(): jnp.dot(normed, matrix, preferred_element_type=jnp.float32)  8.4 us
    all_to_all x1, waiting for transfers between devices, copy_for_each(): lax.all_to_all(jnp.broadcast_to(array[None], (size, *array.shape)), axis,...  7.99 us
    unnamed x23, local copies, waits for them, and re-layouts  7.05 us
    ppermute x1, starting transfers between devices, shifted(): return lax.ppermute(block, axis, route)  5.78 us
    all_to_all x1, starting transfers between devices, copy_for_each(): lax.all_to_all(jnp.broadcast_to(array[None], (size, *array.shape)), axis,...  4.83 us
    dot_general x1, matrix products, local(): jnp.dot(merged, out_weight, preferred_element_type=jnp.float32)  4.36 us
  transfers between devices with their start and end apart: 3, of which 2 were waited for; matrix products, arithmetic and copies ran while one was open for 9% of the time, Pallas kernels for 51%

profile of v2, /device:TPU:1, one launch (start us, length us, event | category | flops | bytes accessed | tf_op | source)
XLA Modules:
  0.0 137.2 jit_solution(4841906489871481068)
XLA Ops:
  0.6 0.0 copy-start
  0.6 2.2 %broadcast_in_dim.40 = bf16[4,64,2048]{2,1,0:T(8,128)(2,1)} broadcast(bf16[64,2048]{1,0:T(8,128)(2,1)} %param.12), dimensions={1,2} | broadcast | bytes 1310720 | tf_op jit(solution)/shard_map/broadcast_in_dim | solution.py:24
  2.8 4.8 %all-to-all-start = ((bf16[4,64,2048]{2,1,0:T(8,128)(2,1)}), bf16[4,64,2048]{2,1,0:T(8,128)(2,1)S(1)}, u32[]{:S(2)}, u32[]{:S(2)}) async-start(bf16[4,64,2048]{2,1,0:T(8,128)(2,1)} %broadcast_in_dim.40), calls=%async_computation | async-start | bytes 2097152 | tf_op jit(solution)/shard_map/all_to_all | solution.py:23
  7.7 5.3 %copy.24 = bf16[256,8,2,512]{3,1,2,0:T(8,128)(2,1)} copy(bf16[256,8,2,512]{3,2,1,0:T(2,128)(2,1)} %bitcast.65) | data formatting | bytes 8388608
  13.0 8.0 %all-to-all-done = bf16[4,64,2048]{2,1,0:T(8,128)(2,1)S(1)} async-done(((bf16[4,64,2048]{2,1,0:T(8,128)(2,1)}), bf16[4,64,2048]{2,1,0:T(8,128)(2,1)S(1)}, u32[]{:S(2)}, u32[]{:S(2)}) %all-to-all-start) | async-done | bytes 1048608 | tf_op jit(solution)/shard_map/all_to_all | solution.py:23
  21.0 0.3 fusion
  21.3 0.3 fusion.2
  21.6 1.0 copy-done.1
  22.6 1.5 %fusion.17 = bf16[256,512]{1,0:T(8,128)(2,1)} fusion(bf16[256,2048]{1,0:T(8,128)(2,1)S(1)} %bitcast.60, bf16[256,8,4,128]{3,2,1,0:T(4,128)(2,1)S(1)} %bitcast.70), kind=kOutput, calls=%fused_computation.18 | convolution fusion | flops 537133056 | bytes 3407872 | tf_op jit(solution)/shard_map/dot_general | solution.py:407
  24.1 1.2 copy.19
  25.2 0.0 copy-start.9
  25.2 1.9 %convolution_convert_fusion.3.k_ref = bf16[256,128]{1,0:T(8,128)(2,1)S(1)} fusion(bf16[256,2048]{1,0:T(8,128)(2,1)} %bitcast.61, bf16[2048,1,128]{2,0,1:T(8,128)(2,1)} %param.15), kind=kOutput, calls=%fused_computation.20 | convolution fusion | flops 134250496 | bytes 1638400 | tf_op jit(solution)/shard_map/dot_general | solution.py:407
  27.2 2.2 %convolution_convert_fusion.2 = bf16[256,128]{1,0:T(8,128)(2,1)} fusion(bf16[256,2048]{1,0:T(8,128)(2,1)S(1)} %bitcast.62, bf16[2048,1,128]{2,0,1:T(8,128)(2,1)} %param.16), kind=kOutput, calls=%fused_computation.19 | convolution fusion | flops 134250496 | bytes 1638400 | tf_op jit(solution)/shard_map/dot_general | solution.py:407
  29.4 0.7 fusion.11
  30.1 0.0 copy-start.4
  30.2 0.7 copy-done.4
  30.9 5.8 %collective-permute-start = (bf16[16,512]{1,0:T(8,128)(2,1)S(1)}, bf16[16,512]{1,0:T(8,128)(2,1)S(1)}, u32[]{:S(2)}, u32[]{:S(2)}) collective-permute-start(bf16[16,512]{1,0:T(8,128)(2,1)S(1)} %slice.96), channel_id=1, source_target_pairs={{0,4},{4,8},{8,12},{12,16},{16,20},{20,24},{24,28},{28,32},{32,36}... | collective-permute-start | bytes 49160 | tf_op jit(solution)/shard_map/ppermute | solution.py:31
  36.7 2.1 %convolution_convert_fusion.1 = bf16[256,1024]{1,0:T(8,128)(2,1)} fusion(bf16[256,2048]{1,0:T(8,128)(2,1)S(1)} %bitcast.64, bf16[2048,1024]{1,0:T(8,128)(2,1)S(1)} %bitcast.66), kind=kOutput, calls=%fused_computation.11 | convolution fusion | flops 1074003968 | bytes 5767168 | tf_op jit(solution)/shard_map/dot_general | solution.py:407
  38.7 1.5 %reshape.122 = bf16[256,2,512]{2,1,0:T(2,128)(2,1)S(1)} reshape(bf16[256,1024]{1,0:T(8,128)(2,1)} %convolution_convert_fusion.1) | data formatting | bytes 1048576 | tf_op jit(solution)/shard_map/reshape | solution.py:417
  40.2 0.0 copy-start.10
  40.2 1.6 %fusion.99 = (bf16[256,1,512]{2,1,0:T(2,128)(2,1)S(1)}, bf16[256,1,512]{2,1,0:T(2,128)(2,1)}) fusion(bf16[256,2,512]{2,1,0:T(2,128)(2,1)S(1)} %reshape.122), kind=kLoop, calls=%fused_computation.101 | loop fusion | bytes 1048576 | tf_op jit(solution)/shard_map/slice | solution.py:433
  41.8 0.9 copy.20
  42.8 0.1 broadcast_in_dim.41.lam_ref
  42.9 0.1 broadcast_in_dim.42.gain_ref
  42.9 69.6 %attend.1 = (bf16[2,128,512]{2,1,0:T(8,128)(2,1)S(1)}, f32[2,2,4,128]{3,2,1,0:T(4,128)S(1)}) custom-call(bf16[4,128,128]{2,1,0:T(8,128)(2,1)S(1)} %get-tuple-element.9.q_ref, bf16[4,128,128]{2,1,0:T(8,128)(2,1)S(1)} %get-tuple-element.8.qs_ref, bf16[256,128]{1,0:T(8,128)(2,1)S(1)} %convolution_convert_fusion.3.k_ref, bf16[256,128]{1,0:T(8,128)(2,1)S(1)} %bitcast.58, ...), custom_call_target="tpu_custom_call" | custom-call | tf_op jit(solution)/shard_map/attend/pallas_call | solution.py:337
  112.6 0.0 collective-permute-done
  112.6 1.0 maximum_convert_fusion
  113.6 4.4 %convolution_convert_fusion = bf16[256,2048]{1,0:T(8,128)(2,1)} fusion(bf16[512,2048]{1,0:T(8,128)(2,1)S(1)} %copy-done, bf16[256,512]{1,0:T(8,128)(2,1)S(1)} %bitcast.59, bf16[1,512,512]{2,1,0:T(8,128)(2,1)} %param.20, bf16[256,512]{1,0:T(8,128)(2,1)} %copy-done.4, f32[272,512]{1,0:T(8,128)S(1)} %maximum_convert_fusion, ...), kind=kOutput, calls=%fused_computation.2 | convolution fusion | flops 678035456 | bytes 13372432 | tf_op jit(solution)/shard_map/dot_general | solution.py:437
  118.0 3.5 %all-to-all-start.1 = ((bf16[4,64,2048]{2,1,0:T(8,128)(2,1)}), bf16[4,64,2048]{2,1,0:T(8,128)(2,1)S(1)}, u32[]{:S(2)}, u32[]{:S(2)}) async-start(bf16[4,64,2048]{2,1,0:T(8,128)(2,1)} %bitcast.67), calls=%async_computation.1 | async-start | bytes 2097152 | tf_op jit(solution)/shard_map/all_to_all | solution.py:36
  121.5 0.6 pad_maximum_fusion
  122.1 14.1 %all-to-all-done.1 = bf16[4,64,2048]{2,1,0:T(8,128)(2,1)S(1)} async-done(((bf16[4,64,2048]{2,1,0:T(8,128)(2,1)}), bf16[4,64,2048]{2,1,0:T(8,128)(2,1)S(1)}, u32[]{:S(2)}, u32[]{:S(2)}) %all-to-all-start.1) | async-done | bytes 1048608 | tf_op jit(solution)/shard_map/all_to_all | solution.py:36
  136.3 0.9 reduce_sum.22
  (21 shorter events, 0.1 us)
Async XLA Ops:
  0.6 113.0 %copy-start = (bf16[512,2048]{1,0:T(8,128)(2,1)S(1)}, bf16[512,2048]{1,0:T(8,128)(2,1)}, u32[]{:S(2)}) copy-start(bf16[512,2048]{1,0:T(8,128)(2,1)} %param.23) | copy-start | bytes 6291460
  2.8 18.2 %all-to-all-start = ((bf16[4,64,2048]{2,1,0:T(8,128)(2,1)}), bf16[4,64,2048]{2,1,0:T(8,128)(2,1)S(1)}, u32[]{:S(2)}, u32[]{:S(2)}) async-start(bf16[4,64,2048]{2,1,0:T(8,128)(2,1)} %broadcast_in_dim.40), calls=%async_computation | async-start | bytes 2097152 | tf_op jit(solution)/shard_map/all_to_all | solution.py:23
  7.7 13.6 %copy-start.5 = (f32[2048]{0:T(1024)S(1)}, f32[2048]{0:T(1024)}, u32[]{:S(2)}) copy-start(f32[2048]{0:T(1024)} %param.13) | copy-start | bytes 24580
  21.0 1.6 %copy-start.8 = (bf16[2048,4,128]{2,1,0:T(4,128)(2,1)S(1)}, bf16[2048,4,128]{2,1,0:T(4,128)(2,1)}, u32[]{:S(2)}) copy-start(bf16[2048,4,128]{2,1,0:T(4,128)(2,1)} %param.14) | copy-start | bytes 6291460
  21.6 1.0 copy-start.1
  24.1 3.1 %copy-start.2 = (bf16[4,64,2048]{2,1,0:T(8,128)(2,1)S(1)}, bf16[4,64,2048]{2,1,0:T(8,128)(2,1)}, u32[]{:S(2)}) copy-start(bf16[4,64,2048]{2,1,0:T(8,128)(2,1)} %copy-done.1) | copy-start | bytes 3145732
  25.2 4.2 %copy-start.9 = (bf16[2048,1,512]{2,0,1:T(8,128)(2,1)S(1)}, bf16[2048,1,512]{2,0,1:T(8,128)(2,1)}, u32[]{:S(2)}) copy-start(bf16[2048,1,512]{2,0,1:T(8,128)(2,1)} %param.19) | copy-start | bytes 6291460
  27.2 9.5 %copy-start.3 = (bf16[256,8,2,512]{3,1,2,0:T(8,128)(2,1)S(1)}, bf16[256,8,2,512]{3,1,2,0:T(8,128)(2,1)}, u32[]{:S(2)}) copy-start(bf16[256,8,2,512]{3,1,2,0:T(8,128)(2,1)} %copy.24) | copy-start | bytes 12582916
  30.1 0.7 copy-start.4
  30.9 81.7 %collective-permute-start = (bf16[16,512]{1,0:T(8,128)(2,1)S(1)}, bf16[16,512]{1,0:T(8,128)(2,1)S(1)}, u32[]{:S(2)}, u32[]{:S(2)}) collective-permute-start(bf16[16,512]{1,0:T(8,128)(2,1)S(1)} %slice.96), channel_id=1, source_target_pairs={{0,4},{4,8},{8,12},{12,16},{16,20},{20,24},{24,28},{28,32},{32,36}... | collective-permute-start | bytes 49160 | tf_op jit(solution)/shard_map/ppermute | solution.py:31
  38.7 4.0 %copy-start.7 = (f32[4]{0:T(128)S(1)}, f32[4]{0:T(128)}, u32[]{:S(2)}) copy-start(f32[4]{0:T(128)} %param.17) | copy-start | bytes 52
  38.7 4.1 %copy-start.6 = (f32[128]{0:T(128)S(1)}, f32[128]{0:T(128)}, u32[]{:S(2)}) copy-start(f32[128]{0:T(128)} %param.18) | copy-start | bytes 1540
  40.2 73.4 %copy-start.10 = (f32[1,512]{1,0:T(1,128)S(1)}, f32[1,512]{1,0:T(1,128)}, u32[]{:S(2)}) copy-start(f32[1,512]{1,0:T(1,128)} %param.21) | copy-start | bytes 6148
  118.0 18.3 %all-to-all-start.1 = ((bf16[4,64,2048]{2,1,0:T(8,128)(2,1)}), bf16[4,64,2048]{2,1,0:T(8,128)(2,1)S(1)}, u32[]{:S(2)}, u32[]{:S(2)}) async-start(bf16[4,64,2048]{2,1,0:T(8,128)(2,1)} %bitcast.67), calls=%async_computation.1 | async-start | bytes 2097152 | tf_op jit(solution)/shard_map/all_to_all | solution.py:36

commit v3 on v2

--- a/solution.py
+++ b/solution.py
@@ -25,27 +25,162 @@
     )
 
 
-def shifted(block, axis, distance):
-    devices = range(lax.axis_size(axis))
-    route = [(i - distance, i) for i in devices if i - distance in devices]
-    return lax.ppermute(block, axis, route)
-
-
-def sent_and_summed(array, axis):
-    size = lax.axis_size(axis)
-    pieces = lax.all_to_all(array.reshape(size, -1, array.shape[1]), axis, 0, 0, tiled=True)
-    return jnp.sum(pieces.astype(jnp.float32), axis=0)
+def project_kernel(
+    tok_ref, gain_ref, wq, wk, wv, wp, wg,
+    q_own, q_far, k_ref, vt_ref, pool_ref, rim_ref, gate_ref,
+    normed, vq, vk, vv, vp, vg, sems,
+):
+    copies = [
+        pltpu.make_async_copy(src, dst, sems.at[n])
+        for n, (src, dst) in enumerate(((wk, vk), (wv, vv), (wq, vq), (wp, vp), (wg, vg)))
+    ]
+    for copy in copies:
+        copy.start()
+    gain = gain_ref[...]
+    for b in range(0, ROWS, 32):
+        x = tok_ref[b:b + 32, :].astype(jnp.float32)
+        scale = lax.rsqrt(jnp.mean(x * x, axis=1, keepdims=True) + NORM_EPS)
+        normed[b:b + 32, :] = (x * scale * gain).astype(jnp.bfloat16)
+
+    def project(weight):
+        return jnp.dot(normed[...], weight, preferred_element_type=jnp.float32)
+
+    copies[0].wait()
+    k_ref[...] = project(vk[...]).astype(jnp.bfloat16)
+    copies[1].wait()
+    v = project(vv[...])
+    for b in (0, HALF):
+        vt_ref[b:b + HALF, :] = v[b:b + HALF].T.astype(jnp.bfloat16)
+    copies[2].wait()
+    for h in range(4):
+        q = project(vq[:, h * 128:(h + 1) * 128]) * 0.125
+        q_own[h] = q[:HALF].T.astype(jnp.bfloat16)
+        q_far[h] = q[HALF:].T.astype(jnp.bfloat16)
+    copies[3].wait()
+    pool_in = project(vp[...]).astype(jnp.bfloat16)
+    pool_ref[...] = pool_in
+    rim_ref[...] = pool_in[ROWS - WINDOW:]
+    copies[4].wait()
+    for g in (0, 1):
+        gate_ref[g] = project(vg[g]).astype(jnp.bfloat16)
+
+
+def project(rows, norm_gain, wq, wk, wv, wp, wg):
+    bf = jnp.bfloat16
+    vmem = pl.BlockSpec(memory_space=pltpu.VMEM)
+    anywhere = pl.BlockSpec(memory_space=pl.ANY)
+    shape = jax.ShapeDtypeStruct
+    return pl.pallas_call(
+        project_kernel,
+        out_shape=(
+            shape((4, 128, HALF), bf), shape((4, 128, HALF), bf),
+            shape((ROWS, 128), bf), shape((ROWS, 128), bf),
+            shape((ROWS, 512), bf), shape((WINDOW, 512), bf), shape((2, ROWS, 512), bf),
+        ),
+        in_specs=[vmem, vmem] + [anywhere] * 5,
+        out_specs=(vmem,) * 7,
+        scratch_shapes=[
+            pltpu.VMEM((ROWS, 2048), bf),
+            pltpu.VMEM(wq.shape, bf), pltpu.VMEM(wk.shape, bf), pltpu.VMEM(wv.shape, bf),
+            pltpu.VMEM(wp.shape, bf), pltpu.VMEM(wg.shape, bf),
+            pltpu.SemaphoreType.DMA((5,)),
+        ],
+        compiler_params=pltpu.CompilerParams(vmem_limit_bytes=48 * 2**20),
+        cost_estimate=pl.CostEstimate(
+            flops=2 * ROWS * 2048 * 2304, bytes_accessed=10**7, transcendentals=0
+        ),
+        name="project",
+    )(rows, norm_gain[None], wq, wk, wv, wp, wg)
+
+
+def output_kernel(
+    att_ref, gate_ref, pool_ref, rim_ref, mix_ref, scale_ref, weight_ref,
+    out_ref,
+    merged, part, got, s_sem, r_sem,
+):
+    x = lax.axis_index("tp")
+    peers = [{"tp": lax.rem(x + d, 4)} for d in (1, 2, 3)]
+    barrier = pltpu.get_barrier_semaphore()
+    for peer in peers:
+        pl.semaphore_signal(barrier, inc=1, device_id=peer, device_id_type=MESH)
+
+    f32, bf = jnp.float32, jnp.bfloat16
+    for cb in range(0, 512, 128):
+        cols = slice(cb, cb + 128)
+        own = pool_ref[:, cols].astype(f32)
+        rim = jnp.where(lax.axis_index("sp") == 0, 0.0, rim_ref[:, cols].astype(f32))
+        sums = jnp.concatenate([rim, own], axis=0)
+        picked = sums
+        for n, shift in enumerate((1, 2, 4, 8)):
+            sums = sums + pltpu.roll(sums, shift, 0)
+            picked = jnp.where(x >= n, sums, picked)
+        position = lax.axis_index("sp") * ROWS + lax.broadcasted_iota(jnp.int32, (ROWS, 128), 0)
+        span = jnp.left_shift(jnp.int32(2), x)
+        counts = jnp.minimum(position + 1, span).astype(f32)
+        merged[:, cols] = (picked[WINDOW:] / counts - own).astype(bf)
+    pool_out = jnp.dot(merged[...], mix_ref[...], preferred_element_type=f32) * scale_ref[...]
+    attended = jnp.concatenate([att_ref[0], att_ref[1]], axis=0).astype(f32)
+    merged[...] = (
+        jax.nn.sigmoid(gate_ref[0].astype(f32)) * attended
+        + jax.nn.sigmoid(gate_ref[1].astype(f32)) * pool_out
+    ).astype(bf)
+
+    def partial(d):
+        first = pl.multiple_of(lax.rem(x + d, 4) * 64, 64)
+        return jnp.dot(merged[pl.ds(first, 64), :], weight_ref[...], preferred_element_type=f32)
+
+    def send(d):
+        return pltpu.make_async_remote_copy(
+            src_ref=part.at[d - 1], dst_ref=got.at[d - 1],
+            send_sem=s_sem.at[d - 1], recv_sem=r_sem.at[d - 1],
+            device_id=peers[d - 1], device_id_type=MESH,
+        )
+
+    part[1] = partial(2).astype(bf)
+    pl.semaphore_wait(barrier, 3)
+    part[0] = partial(1).astype(bf)
+    send(2).start()
+    part[2] = partial(3).astype(bf)
+    send(1).start()
+    total = partial(0).astype(bf).astype(f32)
+    send(3).start()
+    for d in (1, 3, 2):
+        send(d).wait()
+        total = total + got[d - 1].astype(f32)
+    out_ref[...] = total.astype(bf)
+
+
+def output(att, gates, pool_in, rim, mix, scale, weight):
+    bf = jnp.bfloat16
+    vmem = pl.BlockSpec(memory_space=pltpu.VMEM)
+    dma = pltpu.SemaphoreType.DMA
+    return pl.pallas_call(
+        output_kernel,
+        out_shape=jax.ShapeDtypeStruct((64, 2048), bf),
+        in_specs=[vmem] * 7,
+        out_specs=vmem,
+        scratch_shapes=[
+            pltpu.VMEM((ROWS, 512), bf),
+            pltpu.VMEM((3, 64, 2048), bf),
+            pltpu.VMEM((3, 64, 2048), bf),
+            dma((3,)), dma((3,)),
+        ],
+        compiler_params=pltpu.CompilerParams(
+            collective_id=1, has_side_effects=True, vmem_limit_bytes=32 * 2**20
+        ),
+        name="output",
+    )(att, gates, pool_in, rim, mix, scale, weight)
 
 
 def attention_kernel(
-    q_ref, qs_ref, k_ref, v_ref, lam_ref, gain_ref,
-    att_ref, lse_ref,
-    kv, qbd, qin, m_ref, acc_ref, attx, lsex, attr, lser,
+    q_ref, qs_ref, k_ref, v_ref, rim_ref, lam_ref, gain_ref,
+    att_ref, lse_ref, rim_out,
+    kv, qbd, qin, m_ref, acc_ref, attx, lsex, attr, lser, rim_in,
     *rest,
 ):
     sb, pb, bm = rest[:NB], rest[NB:2 * NB], rest[2 * NB:3 * NB]
     (own_sem, y_s, y_r, vy_s, vy_r, z_s, z_r,
-     sib_s, sib_r, q_s, q_r, o_s, o_r) = rest[3 * NB:]
+     sib_s, sib_r, q_s, q_r, o_s, o_r, rim_s, rim_r) = rest[3 * NB:]
     me = lax.axis_index("sp")
     z, y, c = me // (NY * NC), (me // NC) % NY, me % NC
 
@@ -58,7 +193,9 @@
     y_peers = [at(z, (y + d) % NY, c) for d in (1, 2, 3)]
 
     barrier = pltpu.get_barrier_semaphore()
-    peers = [sibling, partner, *z_next, *y_peers]
+    n_sp = NZ * NY * NC
+    after, before = {"sp": lax.rem(me + 1, n_sp)}, {"sp": lax.rem(me + n_sp - 1, n_sp)}
+    peers = [sibling, partner, *z_next, *y_peers, after, before]
     for peer in peers:
         pl.semaphore_signal(barrier, inc=1, device_id=peer, device_id_type=MESH)
     pl.semaphore_wait(barrier, len(peers))
@@ -113,6 +250,8 @@
         z_msg(1, 1, way, 0, v_ref).start()
     q_copy = remote(qs_ref, qin, q_s, q_r, partner)
     q_copy.start()
+    rim_copy = remote(rim_ref, rim_in, rim_s, rim_r, after)
+    rim_copy.start()
     own_k.wait()
     for d in (0, 2, 1):
         k_to_y(0, 0, d).start()
@@ -173,33 +312,40 @@
             values(i), pb[slot][...], preferred_element_type=jnp.float32
         )
 
-    def block(i, tiles, base=None):
-        n = len(tiles)
+    def block(items, base=None):
+        n = len(items)
         for u in range(LAG):
-            scores(i, tiles[u], u % NB, base)
+            scores(*items[u], u % NB, base)
         for u in range(n):
             if u + LAG < n:
-                scores(i, tiles[u + LAG], (u + LAG) % NB, base)
-            weigh(i, tiles[u], u % NB)
+                scores(*items[u + LAG], (u + LAG) % NB, base)
+            weigh(*items[u], u % NB)
 
     p_own = me * ROWS
     p_far = partner["sp"] * ROWS + HALF
     base_lo = jnp.where(is_low, p_own, p_far)
     base_hi = jnp.where(is_low, p_far, p_own)
 
-    def compute(i):
+    def compute(zs, half):
+        i = 2 * zs + half
+        whole = (2 * zs >= lo) & (2 * zs + 1 < hi)
+
         @pl.when(i < lo)
         def _():
-            block(i, list(range(8)))
-
-        @pl.when((i >= lo) & (i < hi))
-        def _():
-            block(i, list(range(4, 8)))
+            block([(i, t) for t in range(8)])
+
+        @pl.when(whole & (half == 1))
+        def _():
+            block([(2 * zs + w, 4 + u) for w in (0, 1) for u in range(4)])
+
+        @pl.when((i >= lo) & (i < hi) & jnp.logical_not(whole))
+        def _():
+            block([(i, 4 + u) for u in range(4)])
 
         @pl.when((i == lo) | (i == hi))
         def _():
             first = jnp.where(i == lo, 0, 4)
-            block(i, [first + u for u in range(4)], jnp.where(i == lo, base_lo, base_hi))
+            block([(i, first + u) for u in range(4)], jnp.where(i == lo, base_lo, base_hi))
 
     def share(k, ways):
         for way in ways:
@@ -265,7 +411,7 @@
 
         @pl.when((r >= 1) & ((way == 0) | (k > 1)))
         def _():
-            compute(far * 2 + (r - 1) // 2)
+            compute(far, (r - 1) // 2)
 
         return carry
 
@@ -275,7 +421,7 @@
     shared(4, (0,))
 
     def last(yy, carry):
-        compute(slab(4, 0) * 2 + yy)
+        compute(slab(4, 0), yy)
         return carry
 
     lax.fori_loop(0, 2, last, 0)
@@ -302,6 +448,8 @@
         copy.start()
 
     q_copy.wait_send()
+    rim_copy.wait()
+    rim_out[...] = rim_in[...]
     for d in range(3):
         v_to_y(d).wait_send()
         k_to_y(0, 0, d).wait_send()
@@ -328,9 +476,7 @@
     lse_ref[1] = lser[...]
 
 
-def attend(queries, keys_own, values_own, lam, head_gain):
-    qt = jnp.transpose(queries * jnp.asarray(0.125, jnp.bfloat16), (1, 2, 0))
-    vt = values_own.reshape(2, HALF, 128).transpose(0, 2, 1).reshape(ROWS, 128)
+def attend(q_own, q_far, keys_own, vt, rim_rows, lam, head_gain):
     bf, f32 = jnp.bfloat16, jnp.float32
     dma = pltpu.SemaphoreType.DMA
     vmem = pl.BlockSpec(memory_space=pltpu.VMEM)
@@ -339,9 +485,10 @@
         out_shape=(
             jax.ShapeDtypeStruct((2, HALF, 512), bf),
             jax.ShapeDtypeStruct((2, 2, 4, HALF), f32),
+            jax.ShapeDtypeStruct((WINDOW, 512), bf),
         ),
-        in_specs=[vmem] * 6,
-        out_specs=(vmem, vmem),
+        in_specs=[vmem] * 7,
+        out_specs=(vmem,) * 3,
         scratch_shapes=[
             pltpu.VMEM((NZ, NC, 2, NY, ROWS, 128), bf),
             pltpu.VMEM((8, 128, 256), bf),
@@ -352,20 +499,24 @@
             pltpu.VMEM((2, 4, HALF), f32),
             pltpu.VMEM((HALF, 512), bf),
             pltpu.VMEM((2, 4, HALF), f32),
+            pltpu.VMEM((WINDOW, 512), bf),
             *[pltpu.VMEM((KB, 256), f32)] * NB,
             *[pltpu.VMEM((KB, 256), bf)] * NB,
             *[pltpu.VMEM((1, 256), f32)] * NB,
             dma((2,)),
             dma((2, 5, 3)), dma((2, 5, 3)), dma((3,)), dma((3,)),
             dma((2, 5, 5)), dma((2, 5, 5)), dma((2, 5)), dma((2, 5)),
-            dma, dma, dma((2,)), dma((2,)),
+            dma, dma, dma((2,)), dma((2,)), dma, dma,
         ],
         compiler_params=pltpu.CompilerParams(
             collective_id=0, has_side_effects=True, vmem_limit_bytes=48 * 2**20
         ),
+        cost_estimate=pl.CostEstimate(
+            flops=2 * 10**10, bytes_accessed=10**6, transcendentals=2 * 10**7
+        ),
         name="attend",
     )(
-        qt[:, :, :HALF], qt[:, :, HALF:], keys_own, vt,
+        q_own, q_far, keys_own, vt, rim_rows,
         jnp.broadcast_to(lam[:, None], (4, HALF)),
         jnp.broadcast_to(head_gain[:, None], (128, HALF)),
     )
@@ -386,58 +537,19 @@
     out_weight,
 ):
     model_width = tokens.shape[1]
-    heads_local = query_weight.shape[1]
-    group_width = pool_weight.shape[2]
-    channels = gate_weight.shape[2]
-    matrices = (
+    rows = copy_for_each(tokens, "tp").reshape(-1, model_width)
+    q_own, q_far, keys_own, vt, pool_in, rim_rows, gates = project(
+        rows,
+        norm_gain,
         query_weight.reshape(model_width, -1),
         key_weight.reshape(model_width, -1),
         value_weight.reshape(model_width, -1),
         pool_weight.reshape(model_width, -1),
-        gate_weight.reshape(model_width, -1),
+        jnp.transpose(gate_weight, (1, 0, 2)),
     )
-    rows = copy_for_each(tokens, "tp").reshape(-1, model_width)
-    inputs = rows.astype(jnp.float32)
-    normed = (
-        inputs
-        * lax.rsqrt(jnp.mean(inputs * inputs, axis=1, keepdims=True) + NORM_EPS)
-        * norm_gain
-    ).astype(jnp.bfloat16)
-    queries, keys_own, values_own, pool_in, gate_pre = [
-        jnp.dot(normed, matrix, preferred_element_type=jnp.float32).astype(jnp.bfloat16)
-        for matrix in matrices
-    ]
-    tok_rows = rows.shape[0]
-    rim_prev = shifted(pool_in[tok_rows - WINDOW :], "sp", 1)
-    att, lse = attend(
-        queries.reshape(tok_rows, heads_local, 128), keys_own, values_own, mix_lambda, head_gain
-    )
-    attended = att.reshape(tok_rows, 512).astype(jnp.float32)
-    log_out = jnp.concatenate([lse[0], lse[1]], axis=2)
-    gate_pre = gate_pre.reshape(tok_rows, 2, channels)
-    positions = lax.axis_index("sp") * tok_rows + jnp.arange(tok_rows, dtype=jnp.int32)
-    extended = jnp.concatenate([rim_prev, pool_in], axis=0).astype(jnp.float32)
-    window_span = jnp.left_shift(jnp.int32(2), lax.axis_index("tp"))
-    window_sum = jnp.zeros((tok_rows, group_width), jnp.float32)
-    for back_rows in range(WINDOW):
-        window_sum = window_sum + jnp.where(
-            back_rows < window_span,
-            extended[WINDOW - back_rows : WINDOW - back_rows + tok_rows],
-            0.0,
-        )
-    counts = jnp.minimum(positions + 1, window_span).astype(jnp.float32)
-    means = window_sum / counts[:, None]
-    pooled = (means - pool_in.astype(jnp.float32)).astype(jnp.bfloat16)
-    group_parts = jnp.dot(pooled, pool_mix[0], preferred_element_type=jnp.float32) * pool_scale[0]
-    merged = (
-        jax.nn.sigmoid(gate_pre[:, 0].astype(jnp.float32)) * attended
-        + jax.nn.sigmoid(gate_pre[:, 1].astype(jnp.float32)) * group_parts
-    ).astype(jnp.bfloat16)
-    mixed = sent_and_summed(
-        jnp.dot(merged, out_weight, preferred_element_type=jnp.float32).astype(jnp.bfloat16),
-        "tp",
-    )
-    return (mixed.astype(jnp.bfloat16), log_out)
+    att, lse, rim = attend(q_own, q_far, keys_own, vt, rim_rows, mix_lambda, head_gain)
+    mixed = output(att, gates, pool_in, rim, pool_mix[0], pool_scale, out_weight)
+    return (mixed, jnp.concatenate([lse[0], lse[1]], axis=2))
 
 
 def solution(mesh):

time: 138 us -> 118 us (0.86)
  the two profiles are of different devices: /device:TPU:1 before, /device:TPU:225 now
where the time goes in v3:
time: 118 us; the launch traced here: 117 us
  Pallas kernels  92.3 us (78%)
  local copies, waits for them, and re-layouts  10.3 us (9%)
  waiting for transfers between devices  8.91 us (8%)
  starting transfers between devices  4.01 us (3%)
    pallas_call x1, Pallas kernels, attend(): pl.pallas_call(attention_kernel, out_shape=(jax.ShapeDtypeStruct((2, HALF...  71.2 us
    pallas_call x1, Pallas kernels, output(): pl.pallas_call(output_kernel, out_shape=jax.ShapeDtypeStruct((64, 2048),...  16.3 us
    all_to_all x1, waiting for transfers between devices, copy_for_each(): lax.all_to_all(jnp.broadcast_to(array[None], (size, *array.shape)), axis,...  8.91 us
    unnamed x21, local copies, waits for them, and re-layouts  8.13 us
    pallas_call x1, Pallas kernels, project(): pl.pallas_call(project_kernel, out_shape=(shape((4, 128, HALF), bf), shap...  4.85 us
    all_to_all x1, starting transfers between devices, copy_for_each(): lax.all_to_all(jnp.broadcast_to(array[None], (size, *array.shape)), axis,...  4.01 us
  transfers between devices with their start and end apart: 1, of which 1 were waited for; matrix products, arithmetic and copies ran while one was open for 5% of the time, Pallas kernels for 0%

profile of v3, /device:TPU:225, one launch (start us, length us, event | category | flops | bytes accessed | tf_op | source)
XLA Modules:
  0.0 116.8 jit_solution(2509035047727945045)
XLA Ops:
  0.6 2.0 %broadcast_in_dim.8 = bf16[4,64,2048]{2,1,0:T(8,128)(2,1)} broadcast(bf16[64,2048]{1,0:T(8,128)(2,1)} %param.12), dimensions={1,2} | broadcast | bytes 1310720 | tf_op jit(solution)/shard_map/broadcast_in_dim | solution.py:24
  2.7 4.0 %all-to-all-start = ((bf16[4,64,2048]{2,1,0:T(8,128)(2,1)}), bf16[4,64,2048]{2,1,0:T(8,128)(2,1)S(1)}, u32[]{:S(2)}, u32[]{:S(2)}) async-start(bf16[4,64,2048]{2,1,0:T(8,128)(2,1)} %broadcast_in_dim.8), calls=%async_computation | async-start | bytes 2097152 | tf_op jit(solution)/shard_map/all_to_all | solution.py:23
  6.7 0.0 copy-start.6
  6.7 5.0 %copy.18 = bf16[2048,2,512]{2,0,1:T(8,128)(2,1)} copy(bf16[2048,2,512]{2,1,0:T(2,128)(2,1)} %param.22) | data formatting | bytes 8388608 | tf_op args[10]
  11.6 0.0 copy-done.6
  11.6 0.0 copy-start.4
  11.6 0.4 copy.19
  12.0 8.9 %all-to-all-done = bf16[4,64,2048]{2,1,0:T(8,128)(2,1)S(1)} async-done(((bf16[4,64,2048]{2,1,0:T(8,128)(2,1)}), bf16[4,64,2048]{2,1,0:T(8,128)(2,1)S(1)}, u32[]{:S(2)}, u32[]{:S(2)}) %all-to-all-start) | async-done | bytes 1048608 | tf_op jit(solution)/shard_map/all_to_all | solution.py:23
  20.9 0.0 copy-done.4
  20.9 0.0 copy-start.1
  20.9 1.0 copy-done.1
  22.0 0.0 copy-start.2
  22.0 1.0 copy-done.2
  23.0 0.0 copy-start.7
  23.0 0.0 copy-start.8
  23.0 4.8 %project.1 = (bf16[4,128,128]{2,1,0:T(8,128)(2,1)S(1)}, bf16[4,128,128]{2,1,0:T(8,128)(2,1)S(1)}, bf16[256,128]{1,0:T(8,128)(2,1)S(1)}, bf16[256,128]{1,0:T(8,12...) custom-call(bf16[256,2048]{1,0:T(8,128)(2,1)S(1)} %bitcast.18, ...), custom_call_target="tpu_custom_call" | custom-call | flops 2415919104 | bytes 10000000 | tf_op jit(solution)/shard_map/project/pallas_call | solution.py:73
  27.9 0.0 copy-done.7
  27.9 0.1 broadcast_in_dim.11.gain_ref
  27.9 0.0 copy-done.8
  28.0 0.1 broadcast_in_dim.10.lam_ref
  28.0 0.0 copy-start
  28.0 0.0 copy-start.3
  28.0 0.0 copy-start.5
  28.0 71.2 %attend.1 = (bf16[2,128,512]{2,1,0:T(8,128)(2,1)S(1)}, f32[2,2,4,128]{3,2,1,0:T(4,128)S(1)}, bf16[16,512]{1,0:T(8,128)(2,1)S(1)}) custom-call(bf16[4,128,128]{2,1,0:T(8,128)(2,1)S(1)} %get-tuple-element.12.q_ref, bf16[4,128,128]{2,1,0:T(8,128)(2,1)S(1)} %get-tuple-element.13.qs_ref, bf16[256,128]{1,0:T(8,128)(2,1)S(1)} %get-tuple-element.14.k_ref, ...), custom_call_target="tpu_custom_call" | custom-call | flops 20000000000 | bytes 1000000 | tf_op jit(solution)/shard_map/attend/pallas_call | solution.py:483
  99.2 0.0 copy-done
  99.2 0.0 copy-done.3
  99.2 0.0 copy-done.5
  99.2 16.3 %output.1 = bf16[64,2048]{1,0:T(8,128)(2,1)S(1)} custom-call(bf16[2,128,512]{2,1,0:T(8,128)(2,1)S(1)} %get-tuple-element.17.att_ref, bf16[2,256,512]{2,1,0:T(8,128)(2,1)S(1)} %get-tuple-element.18.gate_ref, bf16[256,512]{1,0:T(8,128)(2,1)S(1)} %get-tuple-element.19.pool_ref, bf16[16,512]{1,0:T(8,128)(2,1)S(1)} %get-tuple-element.20.rim_ref, ...), custom_call_target="tpu_custom_call" | custom-call | tf_op jit(solution)/shard_map/output/pallas_call | solution.py:157
  115.5 0.6 pad_maximum_fusion
  116.1 0.7 copy.21
  (1 shorter events, 0.0 us)
Async XLA Ops:
  2.7 18.3 %all-to-all-start = ((bf16[4,64,2048]{2,1,0:T(8,128)(2,1)}), bf16[4,64,2048]{2,1,0:T(8,128)(2,1)S(1)}, u32[]{:S(2)}, u32[]{:S(2)}) async-start(bf16[4,64,2048]{2,1,0:T(8,128)(2,1)} %broadcast_in_dim.8), calls=%async_computation | async-start | bytes 2097152 | tf_op jit(solution)/shard_map/all_to_all | solution.py:23
  6.7 5.0 %copy-start.6 = (bf16[2048,4,128]{2,1,0:T(4,128)(2,1)S(1)}, bf16[2048,4,128]{2,1,0:T(4,128)(2,1)}, u32[]{:S(2)}) copy-start(bf16[2048,4,128]{2,1,0:T(4,128)(2,1)} %param.14) | copy-start | bytes 6291460
  11.6 9.3 %copy-start.4 = (f32[2048]{0:T(1024)S(1)}, f32[2048]{0:T(1024)}, u32[]{:S(2)}) copy-start(f32[2048]{0:T(1024)} %param.13) | copy-start | bytes 24580
  20.9 1.0 copy-start.1
  22.0 1.0 copy-start.2
  23.0 4.9 %copy-start.7 = (f32[128]{0:T(128)S(1)}, f32[128]{0:T(128)}, u32[]{:S(2)}) copy-start(f32[128]{0:T(128)} %param.18) | copy-start | bytes 1540
  23.0 4.9 %copy-start.8 = (f32[4]{0:T(128)S(1)}, f32[4]{0:T(128)}, u32[]{:S(2)}) copy-start(f32[4]{0:T(128)} %param.17) | copy-start | bytes 52
  28.0 71.2 %copy-start = (bf16[512,2048]{1,0:T(8,128)(2,1)S(1)}, bf16[512,2048]{1,0:T(8,128)(2,1)}, u32[]{:S(2)}) copy-start(bf16[512,2048]{1,0:T(8,128)(2,1)} %weight_ref.1) | copy-start | bytes 6291460
  28.0 71.2 %copy-start.3 = (bf16[1,512,512]{2,1,0:T(8,128)(2,1)S(1)}, bf16[1,512,512]{2,1,0:T(8,128)(2,1)}, u32[]{:S(2)}) copy-start(bf16[1,512,512]{2,1,0:T(8,128)(2,1)} %param.20) | copy-start | bytes 1572868
  28.0 71.2 %copy-start.5 = (f32[1,512]{1,0:T(1,128)S(1)}, f32[1,512]{1,0:T(1,128)}, u32[]{:S(2)}) copy-start(f32[1,512]{1,0:T(1,128)} %scale_ref.1) | copy-start | bytes 6148

commit v4 on v3

--- a/solution.py
+++ b/solution.py
@@ -175,12 +175,12 @@
 def attention_kernel(
     q_ref, qs_ref, k_ref, v_ref, rim_ref, lam_ref, gain_ref,
     att_ref, lse_ref, rim_out,
-    kv, qbd, qin, m_ref, acc_ref, attx, lsex, attr, lser, rim_in,
+    kv, qbd, m_ref, acc_ref, rim_in,
     *rest,
 ):
     sb, pb, bm = rest[:NB], rest[NB:2 * NB], rest[2 * NB:3 * NB]
     (own_sem, y_s, y_r, vy_s, vy_r, z_s, z_r,
-     sib_s, sib_r, q_s, q_r, o_s, o_r, rim_s, rim_r) = rest[3 * NB:]
+     sib_s, sib_r, rim_s, rim_r) = rest[3 * NB:]
     me = lax.axis_index("sp")
     z, y, c = me // (NY * NC), (me // NC) % NY, me % NC
 
@@ -188,14 +188,13 @@
         return {"sp": (zz * NY + yy) * NC + cc}
 
     sibling = at(z, y, 1 - c)
-    partner = at(NZ - 1 - z, NY - 1 - y, c)
     z_next = [at((z + 1) % NZ, y, c), at((z + NZ - 1) % NZ, y, c)]
     y_peers = [at(z, (y + d) % NY, c) for d in (1, 2, 3)]
 
     barrier = pltpu.get_barrier_semaphore()
     n_sp = NZ * NY * NC
     after, before = {"sp": lax.rem(me + 1, n_sp)}, {"sp": lax.rem(me + n_sp - 1, n_sp)}
-    peers = [sibling, partner, *z_next, *y_peers, after, before]
+    peers = [sibling, *z_next, *y_peers, after, before]
     for peer in peers:
         pl.semaphore_signal(barrier, inc=1, device_id=peer, device_id_type=MESH)
     pl.semaphore_wait(barrier, len(peers))
@@ -248,8 +247,6 @@
     for way in (0, 1):
         z_msg(1, 0, way, 0, k_ref).start()
         z_msg(1, 1, way, 0, v_ref).start()
-    q_copy = remote(qs_ref, qin, q_s, q_r, partner)
-    q_copy.start()
     rim_copy = remote(rim_ref, rim_in, rim_s, rim_r, after)
     rim_copy.start()
     own_k.wait()
@@ -259,9 +256,6 @@
 
     m_ref[...] = jnp.full_like(m_ref, NEG)
     acc_ref[...] = jnp.zeros_like(acc_ref)
-    is_low = z < NZ // 2
-    g_own = jnp.where(is_low, 0, 4)
-    g_far = 4 - g_own
 
     def block_diagonal(q):
         top = lax.broadcasted_iota(jnp.int32, (HALF, HALF), 0) < 64
@@ -269,7 +263,8 @@
         return jnp.concatenate([jnp.where(top, q, zero), jnp.where(top, zero, q)], axis=1)
 
     for h in range(4):
-        qbd[g_own + h] = block_diagonal(q_ref[h])
+        qbd[h] = block_diagonal(q_ref[h])
+        qbd[4 + h] = block_diagonal(qs_ref[h])
 
     for r in (2, 4, 3):
         v_from_y(NY - r).wait_recv()
@@ -277,8 +272,6 @@
             z_msg(1, r, way, 0).start()
 
     mine = (z * NY + y) // 2
-    lo = jnp.minimum(mine, 15 - mine)
-    hi = 15 - lo
 
     ones = jnp.ones((16, KB), jnp.bfloat16)
 
@@ -293,9 +286,10 @@
         halves = [v[a:a + HALF] for v in pieces(i, 1) for a in (0, HALF)]
         return jnp.concatenate([jnp.concatenate(halves, axis=1), ones], axis=0)
 
-    def scores(i, t, slot, base=None):
+    def scores(i, t, slot, masked=False):
         s = jnp.dot(keys(i), qbd[t], preferred_element_type=jnp.float32)
-        if base is not None:
+        if masked:
+            base = me * ROWS + t // 4 * HALF
             key_pos = i * KB + lax.broadcasted_iota(jnp.int32, (KB, 2 * HALF), 0)
             row = lax.broadcasted_iota(jnp.int32, (KB, 2 * HALF), 1)
             row_pos = base + jnp.where(row < HALF, row, row - HALF)
@@ -312,40 +306,31 @@
             values(i), pb[slot][...], preferred_element_type=jnp.float32
         )
 
-    def block(items, base=None):
+    def block(items, masked=False):
         n = len(items)
         for u in range(LAG):
-            scores(*items[u], u % NB, base)
+            scores(*items[u], u % NB, masked)
         for u in range(n):
             if u + LAG < n:
-                scores(*items[u + LAG], (u + LAG) % NB, base)
+                scores(*items[u + LAG], (u + LAG) % NB, masked)
             weigh(*items[u], u % NB)
 
-    p_own = me * ROWS
-    p_far = partner["sp"] * ROWS + HALF
-    base_lo = jnp.where(is_low, p_own, p_far)
-    base_hi = jnp.where(is_low, p_far, p_own)
-
     def compute(zs, half):
-        i = 2 * zs + half
-        whole = (2 * zs >= lo) & (2 * zs + 1 < hi)
-
-        @pl.when(i < lo)
+        first = 2 * zs
+        i = first + half
+        whole = first + 1 < mine
+
+        @pl.when(whole & (half == 1))
+        def _():
+            block([(first + w, t) for w in (0, 1) for t in range(8)])
+
+        @pl.when((i < mine) & jnp.logical_not(whole))
         def _():
             block([(i, t) for t in range(8)])
 
-        @pl.when(whole & (half == 1))
-        def _():
-            block([(2 * zs + w, 4 + u) for w in (0, 1) for u in range(4)])
-
-        @pl.when((i >= lo) & (i < hi) & jnp.logical_not(whole))
-        def _():
-            block([(i, 4 + u) for u in range(4)])
-
-        @pl.when((i == lo) | (i == hi))
-        def _():
-            first = jnp.where(i == lo, 0, 4)
-            block([(i, first + u) for u in range(4)], jnp.where(i == lo, base_lo, base_hi))
+        @pl.when(i == mine)
+        def _():
+            block([(i, t) for t in range(8)], True)
 
     def share(k, ways):
         for way in ways:
@@ -399,12 +384,6 @@
             @pl.when(k > 1)
             def _():
                 shared(k - 1, (1,))
-
-            @pl.when(k == 1)
-            def _():
-                q_copy.wait_recv()
-                for h in range(4):
-                    qbd[g_far + h] = block_diagonal(qin[h])
 
         way = lax.rem(r + 1, 2)
         far = lax.rem(z + NZ + jnp.where(way == 0, 1 - k, k - 1), NZ)
@@ -440,14 +419,9 @@
             normed = out * scale * gain_ref[...]
             att_out[:, h * HALF:(h + 1) * HALF] = normed.T.astype(jnp.bfloat16)
 
-    finish(g_far, attx, lsex)
-    finish(g_own, att_ref.at[0], lse_ref.at[0])
-    back = (remote(attx, attr, o_s.at[0], o_r.at[0], partner),
-            remote(lsex, lser, o_s.at[1], o_r.at[1], partner))
-    for copy in back:
-        copy.start()
-
-    q_copy.wait_send()
+    for half in (0, 1):
+        finish(4 * half, att_ref.at[half], lse_ref.at[half])
+
     rim_copy.wait()
     rim_out[...] = rim_in[...]
     for d in range(3):
@@ -470,10 +444,6 @@
     for d in range(3):
         k_to_y(4, 0, d).wait_send()
     to_sibling(4, 0, c).wait_send()
-    for copy in back:
-        copy.wait()
-    att_ref[1] = attr[...]
-    lse_ref[1] = lser[...]
 
 
 def attend(q_own, q_far, keys_own, vt, rim_rows, lam, head_gain):
@@ -492,13 +462,8 @@
         scratch_shapes=[
             pltpu.VMEM((NZ, NC, 2, NY, ROWS, 128), bf),
             pltpu.VMEM((8, 128, 256), bf),
-            pltpu.VMEM((4, 128, 128), bf),
             pltpu.VMEM((8, 1, 256), f32),
             pltpu.VMEM((8, 144, 256), f32),
-            pltpu.VMEM((HALF, 512), bf),
-            pltpu.VMEM((2, 4, HALF), f32),
-            pltpu.VMEM((HALF, 512), bf),
-            pltpu.VMEM((2, 4, HALF), f32),
             pltpu.VMEM((WINDOW, 512), bf),
             *[pltpu.VMEM((KB, 256), f32)] * NB,
             *[pltpu.VMEM((KB, 256), bf)] * NB,
@@ -506,7 +471,7 @@
             dma((2,)),
             dma((2, 5, 3)), dma((2, 5, 3)), dma((3,)), dma((3,)),
             dma((2, 5, 5)), dma((2, 5, 5)), dma((2, 5)), dma((2, 5)),
-            dma, dma, dma((2,)), dma((2,)), dma, dma,
+            dma, dma,
         ],
         compiler_params=pltpu.CompilerParams(
             collective_id=0, has_side_effects=True, vmem_limit_bytes=48 * 2**20

time: 118 us -> 114 us (0.966); the launches traced: 117 us -> 114 us
  Pallas kernels: 92.3 us -> 89.6 us
    pallas_call x1, Pallas kernels: 71.2 us -> 68.4 us  [attend(): pl.pallas_call(attention_kernel, out_shape=(jax.ShapeDtypeStruct((2, HALF...]
where the time goes in v4:
time: 114 us
  Pallas kernels  89.6 us (79%)
  local copies, waits for them, and re-layouts  10.3 us (9%)
  waiting for transfers between devices  8.91 us (8%)
  starting transfers between devices  4.01 us (4%)
    pallas_call x1, Pallas kernels, attend(): pl.pallas_call(attention_kernel, out_shape=(jax.ShapeDtypeStruct((2, HALF...  68.4 us
    pallas_call x1, Pallas kernels, output(): pl.pallas_call(output_kernel, out_shape=jax.ShapeDtypeStruct((64, 2048),...  16.3 us
    all_to_all x1, waiting for transfers between devices, copy_for_each(): lax.all_to_all(jnp.broadcast_to(array[None], (size, *array.shape)), axis,...  8.91 us
    unnamed x21, local copies, waits for them, and re-layouts  8.13 us
    pallas_call x1, Pallas kernels, project(): pl.pallas_call(project_kernel, out_shape=(shape((4, 128, HALF), bf), shap...  4.85 us
    all_to_all x1, starting transfers between devices, copy_for_each(): lax.all_to_all(jnp.broadcast_to(array[None], (size, *array.shape)), axis,...  4.01 us
  transfers between devices with their start and end apart: 1, of which 1 were waited for; matrix products, arithmetic and copies ran while one was open for 5% of the time, Pallas kernels for 0%

profile of v4, /device:TPU:225, one launch (start us, length us, event | category | flops | bytes accessed | tf_op | source)
XLA Modules:
  0.0 114.1 jit_solution(13489882704259567041)
XLA Ops:
  0.6 2.0 %broadcast_in_dim.8 = bf16[4,64,2048]{2,1,0:T(8,128)(2,1)} broadcast(bf16[64,2048]{1,0:T(8,128)(2,1)} %param.12), dimensions={1,2} | broadcast | bytes 1310720 | tf_op jit(solution)/shard_map/broadcast_in_dim | solution.py:24
  2.7 4.0 %all-to-all-start = ((bf16[4,64,2048]{2,1,0:T(8,128)(2,1)}), bf16[4,64,2048]{2,1,0:T(8,128)(2,1)S(1)}, u32[]{:S(2)}, u32[]{:S(2)}) async-start(bf16[4,64,2048]{2,1,0:T(8,128)(2,1)} %broadcast_in_dim.8), calls=%async_computation | async-start | bytes 2097152 | tf_op jit(solution)/shard_map/all_to_all | solution.py:23
  6.7 0.0 copy-start.6
  6.7 5.0 %copy.18 = bf16[2048,2,512]{2,0,1:T(8,128)(2,1)} copy(bf16[2048,2,512]{2,1,0:T(2,128)(2,1)} %param.22) | data formatting | bytes 8388608 | tf_op args[10]
  11.6 0.0 copy-done.6
  11.6 0.0 copy-start.4
  11.6 0.4 copy.19
  12.0 8.9 %all-to-all-done = bf16[4,64,2048]{2,1,0:T(8,128)(2,1)S(1)} async-done(((bf16[4,64,2048]{2,1,0:T(8,128)(2,1)}), bf16[4,64,2048]{2,1,0:T(8,128)(2,1)S(1)}, u32[]{:S(2)}, u32[]{:S(2)}) %all-to-all-start) | async-done | bytes 1048608 | tf_op jit(solution)/shard_map/all_to_all | solution.py:23
  20.9 0.0 copy-done.4
  20.9 0.0 copy-start.1
  20.9 1.0 copy-done.1
  22.0 0.0 copy-start.2
  22.0 1.0 copy-done.2
  23.0 0.0 copy-start.7
  23.0 0.0 copy-start.8
  23.0 4.8 %project.1 = (bf16[4,128,128]{2,1,0:T(8,128)(2,1)S(1)}, bf16[4,128,128]{2,1,0:T(8,128)(2,1)S(1)}, bf16[256,128]{1,0:T(8,128)(2,1)S(1)}, bf16[256,128]{1,0:T(8,12...) custom-call(bf16[256,2048]{1,0:T(8,128)(2,1)S(1)} %bitcast.18, ...), custom_call_target="tpu_custom_call" | custom-call | flops 2415919104 | bytes 10000000 | tf_op jit(solution)/shard_map/project/pallas_call | solution.py:73
  27.9 0.0 copy-done.7
  27.9 0.1 broadcast_in_dim.11.gain_ref
  27.9 0.0 copy-done.8
  28.0 0.1 broadcast_in_dim.10.lam_ref
  28.0 0.0 copy-start
  28.0 0.0 copy-start.3
  28.0 0.0 copy-start.5
  28.0 68.4 %attend.1 = (bf16[2,128,512]{2,1,0:T(8,128)(2,1)S(1)}, f32[2,2,4,128]{3,2,1,0:T(4,128)S(1)}, bf16[16,512]{1,0:T(8,128)(2,1)S(1)}) custom-call(bf16[4,128,128]{2,1,0:T(8,128)(2,1)S(1)} %get-tuple-element.12.q_ref, bf16[4,128,128]{2,1,0:T(8,128)(2,1)S(1)} %get-tuple-element.13.qs_ref, bf16[256,128]{1,0:T(8,128)(2,1)S(1)} %get-tuple-element.14.k_ref, ...), custom_call_target="tpu_custom_call" | custom-call | flops 20000000000 | bytes 1000000 | tf_op jit(solution)/shard_map/attend/pallas_call | solution.py:453
  96.5 0.0 copy-done
  96.5 0.0 copy-done.3
  96.5 0.0 copy-done.5
  96.5 16.3 %output.1 = bf16[64,2048]{1,0:T(8,128)(2,1)S(1)} custom-call(bf16[2,128,512]{2,1,0:T(8,128)(2,1)S(1)} %get-tuple-element.17.att_ref, bf16[2,256,512]{2,1,0:T(8,128)(2,1)S(1)} %get-tuple-element.18.gate_ref, bf16[256,512]{1,0:T(8,128)(2,1)S(1)} %get-tuple-element.19.pool_ref, bf16[16,512]{1,0:T(8,128)(2,1)S(1)} %get-tuple-element.20.rim_ref, ...), custom_call_target="tpu_custom_call" | custom-call | tf_op jit(solution)/shard_map/output/pallas_call | solution.py:157
  112.8 0.6 pad_maximum_fusion
  113.4 0.7 copy.21
  (1 shorter events, 0.0 us)
Async XLA Ops:
  2.7 18.3 %all-to-all-start = ((bf16[4,64,2048]{2,1,0:T(8,128)(2,1)}), bf16[4,64,2048]{2,1,0:T(8,128)(2,1)S(1)}, u32[]{:S(2)}, u32[]{:S(2)}) async-start(bf16[4,64,2048]{2,1,0:T(8,128)(2,1)} %broadcast_in_dim.8), calls=%async_computation | async-start | bytes 2097152 | tf_op jit(solution)/shard_map/all_to_all | solution.py:23
  6.7 5.0 %copy-start.6 = (bf16[2048,4,128]{2,1,0:T(4,128)(2,1)S(1)}, bf16[2048,4,128]{2,1,0:T(4,128)(2,1)}, u32[]{:S(2)}) copy-start(bf16[2048,4,128]{2,1,0:T(4,128)(2,1)} %param.14) | copy-start | bytes 6291460
  11.6 9.3 %copy-start.4 = (f32[2048]{0:T(1024)S(1)}, f32[2048]{0:T(1024)}, u32[]{:S(2)}) copy-start(f32[2048]{0:T(1024)} %param.13) | copy-start | bytes 24580
  20.9 1.0 copy-start.1
  22.0 1.0 copy-start.2
  23.0 4.9 %copy-start.7 = (f32[128]{0:T(128)S(1)}, f32[128]{0:T(128)}, u32[]{:S(2)}) copy-start(f32[128]{0:T(128)} %param.18) | copy-start | bytes 1540
  23.0 4.9 %copy-start.8 = (f32[4]{0:T(128)S(1)}, f32[4]{0:T(128)}, u32[]{:S(2)}) copy-start(f32[4]{0:T(128)} %param.17) | copy-start | bytes 52
  28.0 68.4 %copy-start = (bf16[512,2048]{1,0:T(8,128)(2,1)S(1)}, bf16[512,2048]{1,0:T(8,128)(2,1)}, u32[]{:S(2)}) copy-start(bf16[512,2048]{1,0:T(8,128)(2,1)} %weight_ref.1) | copy-start | bytes 6291460
  28.0 68.5 %copy-start.3 = (bf16[1,512,512]{2,1,0:T(8,128)(2,1)S(1)}, bf16[1,512,512]{2,1,0:T(8,128)(2,1)}, u32[]{:S(2)}) copy-start(bf16[1,512,512]{2,1,0:T(8,128)(2,1)} %param.20) | copy-start | bytes 1572868
  28.0 68.5 %copy-start.5 = (f32[1,512]{1,0:T(1,128)S(1)}, f32[1,512]{1,0:T(1,128)}, u32[]{:S(2)}) copy-start(f32[1,512]{1,0:T(1,128)} %scale_ref.1) | copy-start | bytes 6148

commit v5 on v4

--- a/solution.py
+++ b/solution.py
@@ -85,7 +85,7 @@
             pltpu.VMEM(wp.shape, bf), pltpu.VMEM(wg.shape, bf),
             pltpu.SemaphoreType.DMA((5,)),
         ],
-        compiler_params=pltpu.CompilerParams(vmem_limit_bytes=48 * 2**20),
+        compiler_params=pltpu.CompilerParams(vmem_limit_bytes=50 * 2**20),
         cost_estimate=pl.CostEstimate(
             flops=2 * ROWS * 2048 * 2304, bytes_accessed=10**7, transcendentals=0
         ),
@@ -316,15 +316,9 @@
             weigh(*items[u], u % NB)
 
     def compute(zs, half):
-        first = 2 * zs
-        i = first + half
-        whole = first + 1 < mine
-
-        @pl.when(whole & (half == 1))
-        def _():
-            block([(first + w, t) for w in (0, 1) for t in range(8)])
-
-        @pl.when((i < mine) & jnp.logical_not(whole))
+        i = 2 * zs + half
+
+        @pl.when(i < mine)
         def _():
             block([(i, t) for t in range(8)])
 
@@ -377,6 +371,10 @@
         def _():
             share(k, (0, 1))
 
+        @pl.when((r == 3) & (k == 4))
+        def _():
+            share(4, (0,))
+
         @pl.when(r == 1)
         def _():
             shared(k - 1, (0,))
@@ -396,7 +394,6 @@
 
     share(0, (0,))
     lax.fori_loop(0, 20, tick, 0)
-    share(4, (0,))
     shared(4, (0,))
 
     def last(yy, carry):

time: 114 us -> 110 us (0.965)
  Pallas kernels: 89.6 us -> 87.4 us
  waiting for transfers between devices: 8.91 us -> 7.57 us
    pallas_call x1, Pallas kernels: 68.4 us -> 66.1 us  [attend(): pl.pallas_call(attention_kernel, out_shape=(jax.ShapeDtypeStruct((2, HALF...]
    all_to_all x1, waiting for transfers between devices: 8.91 us -> 7.57 us  [copy_for_each(): lax.all_to_all(jnp.broadcast_to(array[None], (size, *array.shape)), axis,...]
  transfers between devices with their start and end apart: 1 -> 1, of which waited for: 1 -> 1; matrix products, arithmetic and copies ran while one was open for 5% -> 6% of each run, Pallas kernels for 0% -> 0%
where the time goes in v5:
time: 110 us
  Pallas kernels  87.4 us (79%)
  local copies, waits for them, and re-layouts  9.6 us (9%)
  waiting for transfers between devices  7.57 us (7%)
  starting transfers between devices  4.01 us (4%)
    pallas_call x1, Pallas kernels, attend(): pl.pallas_call(attention_kernel, out_shape=(jax.ShapeDtypeStruct((2, HALF...  66.1 us
    pallas_call x1, Pallas kernels, output(): pl.pallas_call(output_kernel, out_shape=jax.ShapeDtypeStruct((64, 2048),...  16.2 us
    all_to_all x1, waiting for transfers between devices, copy_for_each(): lax.all_to_all(jnp.broadcast_to(array[None], (size, *array.shape)), axis,...  7.57 us
    unnamed x21, local copies, waits for them, and re-layouts  7.39 us
    pallas_call x1, Pallas kernels, project(): pl.pallas_call(project_kernel, out_shape=(shape((4, 128, HALF), bf), shap...  5.01 us
    all_to_all x1, starting transfers between devices, copy_for_each(): lax.all_to_all(jnp.broadcast_to(array[None], (size, *array.shape)), axis,...  4.01 us
  transfers between devices with their start and end apart: 1, of which 1 were waited for; matrix products, arithmetic and copies ran while one was open for 6% of the time, Pallas kernels for 0%

profile of v5, /device:TPU:225, one launch (start us, length us, event | category | flops | bytes accessed | tf_op | source)
XLA Modules:
  0.0 109.9 jit_solution(1914562876951003942)
XLA Ops:
  0.6 2.1 %broadcast_in_dim.8 = bf16[4,64,2048]{2,1,0:T(8,128)(2,1)} broadcast(bf16[64,2048]{1,0:T(8,128)(2,1)} %param.12), dimensions={1,2} | broadcast | bytes 1310720 | tf_op jit(solution)/shard_map/broadcast_in_dim | solution.py:24
  2.7 4.0 %all-to-all-start = ((bf16[4,64,2048]{2,1,0:T(8,128)(2,1)}), bf16[4,64,2048]{2,1,0:T(8,128)(2,1)S(1)}, u32[]{:S(2)}, u32[]{:S(2)}) async-start(bf16[4,64,2048]{2,1,0:T(8,128)(2,1)} %broadcast_in_dim.8), calls=%async_computation | async-start | bytes 2097152 | tf_op jit(solution)/shard_map/all_to_all | solution.py:23
  6.7 0.0 copy-start.6
  6.7 5.0 %copy.18 = bf16[2048,2,512]{2,0,1:T(8,128)(2,1)} copy(bf16[2048,2,512]{2,1,0:T(2,128)(2,1)} %param.22) | data formatting | bytes 8388608 | tf_op args[10]
  11.7 0.0 copy-done.6
  11.7 0.0 copy-start.1
  11.7 0.0 copy-start.2
  11.7 0.0 copy-start.4
  11.7 1.7 %copy.19 = bf16[256,8,4,128]{3,1,2,0:T(8,128)(2,1)} copy(bf16[256,8,4,128]{3,2,1,0:T(4,128)(2,1)S(1)} %bitcast.24) | data formatting | bytes 4194304
  13.4 7.6 %all-to-all-done = bf16[4,64,2048]{2,1,0:T(8,128)(2,1)S(1)} async-done(((bf16[4,64,2048]{2,1,0:T(8,128)(2,1)}), bf16[4,64,2048]{2,1,0:T(8,128)(2,1)S(1)}, u32[]{:S(2)}, u32[]{:S(2)}) %all-to-all-start) | async-done | bytes 1048608 | tf_op jit(solution)/shard_map/all_to_all | solution.py:23
  21.0 0.0 copy-done.1
  21.0 0.0 copy-done.2
  21.0 0.0 copy-done.4
  21.0 0.0 copy-start.7
  21.0 0.0 copy-start.8
  21.0 5.0 %project.1 = (bf16[4,128,128]{2,1,0:T(8,128)(2,1)S(1)}, bf16[4,128,128]{2,1,0:T(8,128)(2,1)S(1)}, bf16[256,128]{1,0:T(8,128)(2,1)S(1)}, bf16[256,128]{1,0:T(8,12...) custom-call(bf16[256,2048]{1,0:T(8,128)(2,1)S(1)} %bitcast.17, ...), custom_call_target="tpu_custom_call" | custom-call | flops 2415919104 | bytes 10000000 | tf_op jit(solution)/shard_map/project/pallas_call | solution.py:73
  26.0 0.0 copy-done.7
  26.0 0.1 broadcast_in_dim.11.gain_ref
  26.1 0.0 copy-done.8
  26.1 0.1 broadcast_in_dim.10.lam_ref
  26.2 0.0 copy-start
  26.2 0.0 copy-start.3
  26.2 0.0 copy-start.5
  26.2 66.1 %attend.1 = (bf16[2,128,512]{2,1,0:T(8,128)(2,1)S(1)}, f32[2,2,4,128]{3,2,1,0:T(4,128)S(1)}, bf16[16,512]{1,0:T(8,128)(2,1)S(1)}) custom-call(bf16[4,128,128]{2,1,0:T(8,128)(2,1)S(1)} %get-tuple-element.12.q_ref, bf16[4,128,128]{2,1,0:T(8,128)(2,1)S(1)} %get-tuple-element.13.qs_ref, bf16[256,128]{1,0:T(8,128)(2,1)S(1)} %get-tuple-element.14.k_ref, ...), custom_call_target="tpu_custom_call" | custom-call | flops 20000000000 | bytes 1000000 | tf_op jit(solution)/shard_map/attend/pallas_call | solution.py:450
  92.3 0.0 copy-done
  92.3 0.0 copy-done.3
  92.3 0.0 copy-done.5
  92.3 16.2 %output.1 = bf16[64,2048]{1,0:T(8,128)(2,1)S(1)} custom-call(bf16[2,128,512]{2,1,0:T(8,128)(2,1)S(1)} %get-tuple-element.17.att_ref, bf16[2,256,512]{2,1,0:T(8,128)(2,1)S(1)} %get-tuple-element.18.gate_ref, bf16[256,512]{1,0:T(8,128)(2,1)S(1)} %get-tuple-element.19.pool_ref, bf16[16,512]{1,0:T(8,128)(2,1)S(1)} %get-tuple-element.20.rim_ref, ...), custom_call_target="tpu_custom_call" | custom-call | tf_op jit(solution)/shard_map/output/pallas_call | solution.py:157
  108.6 0.6 pad_maximum_fusion
  109.2 0.7 copy.21
  (1 shorter events, 0.0 us)
Async XLA Ops:
  2.7 18.3 %all-to-all-start = ((bf16[4,64,2048]{2,1,0:T(8,128)(2,1)}), bf16[4,64,2048]{2,1,0:T(8,128)(2,1)S(1)}, u32[]{:S(2)}, u32[]{:S(2)}) async-start(bf16[4,64,2048]{2,1,0:T(8,128)(2,1)} %broadcast_in_dim.8), calls=%async_computation | async-start | bytes 2097152 | tf_op jit(solution)/shard_map/all_to_all | solution.py:23
  6.7 5.0 %copy-start.6 = (bf16[2048,4,128]{2,1,0:T(4,128)(2,1)S(1)}, bf16[2048,4,128]{2,1,0:T(4,128)(2,1)}, u32[]{:S(2)}) copy-start(bf16[2048,4,128]{2,1,0:T(4,128)(2,1)} %param.14) | copy-start | bytes 6291460
  11.7 9.3 %copy-start.1 = (bf16[2048,1,128]{2,0,1:T(8,128)(2,1)S(1)}, bf16[2048,1,128]{2,0,1:T(8,128)(2,1)}, u32[]{:S(2)}) copy-start(bf16[2048,1,128]{2,0,1:T(8,128)(2,1)} %param.15) | copy-start | bytes 1572868
  11.7 9.3 %copy-start.2 = (bf16[2048,1,128]{2,0,1:T(8,128)(2,1)S(1)}, bf16[2048,1,128]{2,0,1:T(8,128)(2,1)}, u32[]{:S(2)}) copy-start(bf16[2048,1,128]{2,0,1:T(8,128)(2,1)} %param.16) | copy-start | bytes 1572868
  11.7 9.3 %copy-start.4 = (f32[2048]{0:T(1024)S(1)}, f32[2048]{0:T(1024)}, u32[]{:S(2)}) copy-start(f32[2048]{0:T(1024)} %param.13) | copy-start | bytes 24580
  21.0 5.0 %copy-start.7 = (f32[128]{0:T(128)S(1)}, f32[128]{0:T(128)}, u32[]{:S(2)}) copy-start(f32[128]{0:T(128)} %param.18) | copy-start | bytes 1540
  21.0 5.1 %copy-start.8 = (f32[4]{0:T(128)S(1)}, f32[4]{0:T(128)}, u32[]{:S(2)}) copy-start(f32[4]{0:T(128)} %param.17) | copy-start | bytes 52
  26.2 66.1 %copy-start = (bf16[512,2048]{1,0:T(8,128)(2,1)S(1)}, bf16[512,2048]{1,0:T(8,128)(2,1)}, u32[]{:S(2)}) copy-start(bf16[512,2048]{1,0:T(8,128)(2,1)} %weight_ref.1) | copy-start | bytes 6291460
  26.2 66.1 %copy-start.3 = (bf16[1,512,512]{2,1,0:T(8,128)(2,1)S(1)}, bf16[1,512,512]{2,1,0:T(8,128)(2,1)}, u32[]{:S(2)}) copy-start(bf16[1,512,512]{2,1,0:T(8,128)(2,1)} %param.20) | copy-start | bytes 1572868
  26.2 66.2 %copy-start.5 = (f32[1,512]{1,0:T(1,128)S(1)}, f32[1,512]{1,0:T(1,128)}, u32[]{:S(2)}) copy-start(f32[1,512]{1,0:T(1,128)} %scale_ref.1) | copy-start | bytes 6148

commit v6 on v5

--- a/solution.py
+++ b/solution.py
@@ -375,6 +375,10 @@
         def _():
             share(4, (0,))
 
+        @pl.when((r == 0) & (k == 1))
+        def _():
+            share(0, (0,))
+
         @pl.when(r == 1)
         def _():
             shared(k - 1, (0,))
@@ -392,7 +396,6 @@
 
         return carry
 
-    share(0, (0,))
     lax.fori_loop(0, 20, tick, 0)
     shared(4, (0,))
 

time: 110 us -> 111 us (level); the launches traced: 110 us -> 109 us
  Pallas kernels: 87.4 us -> 86.2 us
    pallas_call x1, Pallas kernels: 66.1 us -> 65 us  [attend(): pl.pallas_call(attention_kernel, out_shape=(jax.ShapeDtypeStruct((2, HALF...]
where the time goes in v6:
time: 111 us; the launch traced here: 109 us
  Pallas kernels  86.2 us (78%)
  local copies, waits for them, and re-layouts  9.6 us (9%)
  waiting for transfers between devices  7.57 us (7%)
  starting transfers between devices  4.01 us (4%)
    pallas_call x1, Pallas kernels, attend(): pl.pallas_call(attention_kernel, out_shape=(jax.ShapeDtypeStruct((2, HALF...  65 us
    pallas_call x1, Pallas kernels, output(): pl.pallas_call(output_kernel, out_shape=jax.ShapeDtypeStruct((64, 2048),...  16.2 us
    all_to_all x1, waiting for transfers between devices, copy_for_each(): lax.all_to_all(jnp.broadcast_to(array[None], (size, *array.shape)), axis,...  7.57 us
    unnamed x21, local copies, waits for them, and re-layouts  7.39 us
    pallas_call x1, Pallas kernels, project(): pl.pallas_call(project_kernel, out_shape=(shape((4, 128, HALF), bf), shap...  5.01 us
    all_to_all x1, starting transfers between devices, copy_for_each(): lax.all_to_all(jnp.broadcast_to(array[None], (size, *array.shape)), axis,...  4.01 us
  transfers between devices with their start and end apart: 1, of which 1 were waited for; matrix products, arithmetic and copies ran while one was open for 6% of the time, Pallas kernels for 0%

profile of v6, /device:TPU:225, one launch (start us, length us, event | category | flops | bytes accessed | tf_op | source)
XLA Modules:
  0.0 108.7 jit_solution(18061979303441039696)
XLA Ops:
  0.6 2.1 %broadcast_in_dim.8 = bf16[4,64,2048]{2,1,0:T(8,128)(2,1)} broadcast(bf16[64,2048]{1,0:T(8,128)(2,1)} %param.12), dimensions={1,2} | broadcast | bytes 1310720 | tf_op jit(solution)/shard_map/broadcast_in_dim | solution.py:24
  2.7 4.0 %all-to-all-start = ((bf16[4,64,2048]{2,1,0:T(8,128)(2,1)}), bf16[4,64,2048]{2,1,0:T(8,128)(2,1)S(1)}, u32[]{:S(2)}, u32[]{:S(2)}) async-start(bf16[4,64,2048]{2,1,0:T(8,128)(2,1)} %broadcast_in_dim.8), calls=%async_computation | async-start | bytes 2097152 | tf_op jit(solution)/shard_map/all_to_all | solution.py:23
  6.7 0.0 copy-start.6
  6.7 5.0 %copy.18 = bf16[2048,2,512]{2,0,1:T(8,128)(2,1)} copy(bf16[2048,2,512]{2,1,0:T(2,128)(2,1)} %param.22) | data formatting | bytes 8388608 | tf_op args[10]
  11.7 0.0 copy-done.6
  11.7 0.0 copy-start.1
  11.7 0.0 copy-start.2
  11.7 0.0 copy-start.4
  11.7 1.7 %copy.19 = bf16[256,8,4,128]{3,1,2,0:T(8,128)(2,1)} copy(bf16[256,8,4,128]{3,2,1,0:T(4,128)(2,1)S(1)} %bitcast.24) | data formatting | bytes 4194304
  13.4 7.6 %all-to-all-done = bf16[4,64,2048]{2,1,0:T(8,128)(2,1)S(1)} async-done(((bf16[4,64,2048]{2,1,0:T(8,128)(2,1)}), bf16[4,64,2048]{2,1,0:T(8,128)(2,1)S(1)}, u32[]{:S(2)}, u32[]{:S(2)}) %all-to-all-start) | async-done | bytes 1048608 | tf_op jit(solution)/shard_map/all_to_all | solution.py:23
  21.0 0.0 copy-done.1
  21.0 0.0 copy-done.2
  21.0 0.0 copy-done.4
  21.0 0.0 copy-start.7
  21.0 0.0 copy-start.8
  21.0 5.0 %project.1 = (bf16[4,128,128]{2,1,0:T(8,128)(2,1)S(1)}, bf16[4,128,128]{2,1,0:T(8,128)(2,1)S(1)}, bf16[256,128]{1,0:T(8,128)(2,1)S(1)}, bf16[256,128]{1,0:T(8,12...) custom-call(bf16[256,2048]{1,0:T(8,128)(2,1)S(1)} %bitcast.17, ...), custom_call_target="tpu_custom_call" | custom-call | flops 2415919104 | bytes 10000000 | tf_op jit(solution)/shard_map/project/pallas_call | solution.py:73
  26.0 0.0 copy-done.7
  26.0 0.1 broadcast_in_dim.11.gain_ref
  26.1 0.0 copy-done.8
  26.1 0.1 broadcast_in_dim.10.lam_ref
  26.2 0.0 copy-start
  26.2 0.0 copy-start.3
  26.2 0.0 copy-start.5
  26.2 65.0 %attend.1 = (bf16[2,128,512]{2,1,0:T(8,128)(2,1)S(1)}, f32[2,2,4,128]{3,2,1,0:T(4,128)S(1)}, bf16[16,512]{1,0:T(8,128)(2,1)S(1)}) custom-call(bf16[4,128,128]{2,1,0:T(8,128)(2,1)S(1)} %get-tuple-element.12.q_ref, bf16[4,128,128]{2,1,0:T(8,128)(2,1)S(1)} %get-tuple-element.13.qs_ref, bf16[256,128]{1,0:T(8,128)(2,1)S(1)} %get-tuple-element.14.k_ref, ...), custom_call_target="tpu_custom_call" | custom-call | flops 20000000000 | bytes 1000000 | tf_op jit(solution)/shard_map/attend/pallas_call | solution.py:453
  91.2 0.0 copy-done
  91.2 0.0 copy-done.3
  91.2 0.0 copy-done.5
  91.2 16.2 %output.1 = bf16[64,2048]{1,0:T(8,128)(2,1)S(1)} custom-call(bf16[2,128,512]{2,1,0:T(8,128)(2,1)S(1)} %get-tuple-element.17.att_ref, bf16[2,256,512]{2,1,0:T(8,128)(2,1)S(1)} %get-tuple-element.18.gate_ref, bf16[256,512]{1,0:T(8,128)(2,1)S(1)} %get-tuple-element.19.pool_ref, bf16[16,512]{1,0:T(8,128)(2,1)S(1)} %get-tuple-element.20.rim_ref, ...), custom_call_target="tpu_custom_call" | custom-call | tf_op jit(solution)/shard_map/output/pallas_call | solution.py:157
  107.4 0.6 pad_maximum_fusion
  108.0 0.7 copy.21
  (1 shorter events, 0.0 us)
Async XLA Ops:
  2.7 18.3 %all-to-all-start = ((bf16[4,64,2048]{2,1,0:T(8,128)(2,1)}), bf16[4,64,2048]{2,1,0:T(8,128)(2,1)S(1)}, u32[]{:S(2)}, u32[]{:S(2)}) async-start(bf16[4,64,2048]{2,1,0:T(8,128)(2,1)} %broadcast_in_dim.8), calls=%async_computation | async-start | bytes 2097152 | tf_op jit(solution)/shard_map/all_to_all | solution.py:23
  6.7 5.0 %copy-start.6 = (bf16[2048,4,128]{2,1,0:T(4,128)(2,1)S(1)}, bf16[2048,4,128]{2,1,0:T(4,128)(2,1)}, u32[]{:S(2)}) copy-start(bf16[2048,4,128]{2,1,0:T(4,128)(2,1)} %param.14) | copy-start | bytes 6291460
  11.7 9.3 %copy-start.1 = (bf16[2048,1,128]{2,0,1:T(8,128)(2,1)S(1)}, bf16[2048,1,128]{2,0,1:T(8,128)(2,1)}, u32[]{:S(2)}) copy-start(bf16[2048,1,128]{2,0,1:T(8,128)(2,1)} %param.15) | copy-start | bytes 1572868
  11.7 9.3 %copy-start.2 = (bf16[2048,1,128]{2,0,1:T(8,128)(2,1)S(1)}, bf16[2048,1,128]{2,0,1:T(8,128)(2,1)}, u32[]{:S(2)}) copy-start(bf16[2048,1,128]{2,0,1:T(8,128)(2,1)} %param.16) | copy-start | bytes 1572868
  11.7 9.3 %copy-start.4 = (f32[2048]{0:T(1024)S(1)}, f32[2048]{0:T(1024)}, u32[]{:S(2)}) copy-start(f32[2048]{0:T(1024)} %param.13) | copy-start | bytes 24580
  21.0 5.0 %copy-start.7 = (f32[128]{0:T(128)S(1)}, f32[128]{0:T(128)}, u32[]{:S(2)}) copy-start(f32[128]{0:T(128)} %param.18) | copy-start | bytes 1540
  21.0 5.1 %copy-start.8 = (f32[4]{0:T(128)S(1)}, f32[4]{0:T(128)}, u32[]{:S(2)}) copy-start(f32[4]{0:T(128)} %param.17) | copy-start | bytes 52
  26.2 65.0 %copy-start = (bf16[512,2048]{1,0:T(8,128)(2,1)S(1)}, bf16[512,2048]{1,0:T(8,128)(2,1)}, u32[]{:S(2)}) copy-start(bf16[512,2048]{1,0:T(8,128)(2,1)} %weight_ref.1) | copy-start | bytes 6291460
  26.2 65.0 %copy-start.3 = (bf16[1,512,512]{2,1,0:T(8,128)(2,1)S(1)}, bf16[1,512,512]{2,1,0:T(8,128)(2,1)}, u32[]{:S(2)}) copy-start(bf16[1,512,512]{2,1,0:T(8,128)(2,1)} %param.20) | copy-start | bytes 1572868
  26.2 65.0 %copy-start.5 = (f32[1,512]{1,0:T(1,128)S(1)}, f32[1,512]{1,0:T(1,128)}, u32[]{:S(2)}) copy-start(f32[1,512]{1,0:T(1,128)} %scale_ref.1) | copy-start | bytes 6148
